TPU v7x, 256 devices: a 4x2x16 block of a 4x16x16 slice. The times are simulated.
256 devices in a mesh: grp: 2 (over y), ep: 32 (over z, core), tp: 4 (over x).
Axes of the slice: x: 4, y: 2, z: 16, core: 2. Of those that a mesh axis runs over, the one named last changes fastest.
The devices are a block of a 4x16x16 slice.
Arguments:
- mix_rows: bfloat16 [32768, 2048], P(('grp', 'ep', 'tp')), parts along dimension 0, may hold values from -6 to 6
- expert_rows: bfloat16 [32768, 2048], P(('grp', 'ep', 'tp')), parts along dimension 0, may hold values from -6 to 6
- mix_gain: float32 [2048], replicated, may hold values from 0.1 to 1.9
- ffn_gain: float32 [2048], replicated, may hold values from 0.1 to 1.9
- w_query: bfloat16 [2048, 512], P(None, 'tp'), may hold values from -0.125 to 0.125
- w_key: bfloat16 [2048, 512], P(None, 'tp'), may hold values from -0.125 to 0.125
- w_value: bfloat16 [2048, 1024], P(None, 'tp'), may hold values from -0.125 to 0.125
- w_lowrank: bfloat16 [2048, 32], replicated, may hold values from -0.125 to 0.125
- w_decay: bfloat16 [32, 512], replicated, may hold values from -1 to 1
- decay_bias: float32 [512], replicated, may hold values from -1.5 to 16
- decay_shift: float32 [8, 32768], P('tp', ('grp', 'ep')), parts along dimension 1, may hold values from -2 to 0
- head_gain: float32 [128], replicated, may hold values from 0.1 to 1.9
- w_output: bfloat16 [1024, 2048], P('tp'), may hold values from -0.1875 to 0.1875
- route_ids: int32 [32768, 4], P(('grp', 'ep', 'tp')), parts along dimension 0, may hold values from 0 to 127, all different within a row; in each aligned block of 128 rows (0 to 127, 128 to 255, ...) at most 8 rows name the same one
- route_weights: float32 [32768, 4], P(('grp', 'ep', 'tp')), parts along dimension 0, may hold values from 0.3 to 1.2
- w_gate: bfloat16 [128, 2048, 512], P(('ep', 'tp')), may hold values from -0.125 to 0.125
- w_lift: bfloat16 [128, 2048, 512], P(('ep', 'tp')), may hold values from -0.125 to 0.125
- w_drop: bfloat16 [128, 512, 2048], P(('ep', 'tp')), may hold values from -0.25 to 0.25
- shared_gate: bfloat16 [2048, 512], P(None, 'tp'), may hold values from -0.125 to 0.125
- shared_lift: bfloat16 [2048, 512], P(None, 'tp'), may hold values from -0.125 to 0.125
- shared_drop: bfloat16 [512, 2048], P('tp'), may hold values from -0.25 to 0.25
Outputs:
- mixed: bfloat16 [32768, 2048], P(('grp', 'ep', 'tp')), parts along dimension 0
- expert_out: bfloat16 [32768, 2048], P(('grp', 'ep', 'tp')), parts along dimension 0
There are 2 independent parts, one for each index of `grp`. A program takes and returns all parts, laid end to end along the dimension named above; an argument that names none is the same for every part. Nothing has to cross between parts.
Inputs may be any that keep to these rules, and one draw needn't show every extreme that they name: `route_ids`: each row names 4 different experts. In each aligned block of 128 rows (the rows of one device) no expert is named by more than 8 rows.
All inputs are finite; a program needn't handle non-finite values.
Results may differ from a plain program's by a relative error of at most 0.014.
Values may be sent and summed in bfloat16 or wider, within the bound.
A program may use at most 128 MiB of HBM per device.

v0:
```python
import jax
import jax.numpy as jnp
from jax import lax
from jax.sharding import Mesh
from jax.sharding import PartitionSpec as P

DK = 64
DV = 128
BLOCK = 64
EP = ("ep_0", "ep_1")
EP_TP = ("ep_0", "ep_1", "tp")
GRP_EP_TP = ("grp", "ep_0", "ep_1", "tp")
GRP_EP = ("grp", "ep_0", "ep_1")


epsilon = 1e-05
gate_norm = 16.0
highest = lax.Precision.HIGHEST


def filled_with(value, identity):
    return jax.tree.map(
        lambda a, e: jnp.broadcast_to(jnp.asarray(e, a.dtype), a.shape), value, identity
    )


def gathered_once(value, axis):
    leaves = jax.tree.leaves(value)
    sequence = sorted(range(len(leaves)), key=lambda k: -leaves[k].size)
    width = (1, *leaves[sequence[0]].shape)[-1]
    lines = [
        jnp.pad(leaves[k].reshape(-1), (0, -leaves[k].size % width)).reshape(-1, width)
        for k in sequence
    ]
    both, at, found = (lax.all_gather(jnp.concatenate(lines), axis), 0, {})
    for k, line in zip(sequence, lines):
        share = both[:, at : at + len(line)].reshape(len(both), -1)
        found[k] = share[:, : leaves[k].size].reshape(-1, *leaves[k].shape)
        at += len(line)
    numbers = iter(range(len(leaves)))
    return jax.tree.map(lambda _: found[next(numbers)], value)


def carried_in(value, axes, combine, identity):
    before = start = filled_with(value, identity)
    total = value
    for axis in reversed(axes):
        length, mine = (lax.axis_size(axis), lax.axis_index(axis))
        pieces = gathered_once(
            jax.tree.map(lambda part, kind: part.astype(kind), total, (jnp.bfloat16, jnp.bfloat16)),
            axis,
        )
        inside, total = (start, start)
        for k in range(length):
            passed = k < mine
            total = combine(
                total, jax.tree.map(lambda part, own: part[k].astype(own.dtype), pieces, value)
            )
            inside = jax.tree.map(lambda new, old: jnp.where(passed, new, old), total, inside)
        before = combine(inside, before)
    return before


def cut_along(value, dim, length):
    before, after = (value.shape[:dim], value.shape[dim + 1 :])
    return jnp.moveaxis(value.reshape(*before, length, -1, *after), dim, 0)


def in_order(pieces, dim):
    pieces = jnp.moveaxis(pieces, 0, dim)
    dims = pieces.shape
    return pieces.reshape(*dims[:dim], dims[dim] * dims[dim + 1], *dims[dim + 2 :])


def joined_exchange(value, axis, axes, splits, concats):
    sizes = [lax.axis_size(a) for a in axes]
    pieces = cut_along(value, splits[0], sizes[0])
    pieces = jnp.moveaxis(cut_along(pieces, splits[1] + 1, sizes[1]), 0, 1)
    inside = pieces.shape[2:]
    pieces = pieces.reshape(-1, *inside)
    pieces = lax.all_to_all(pieces, axis, split_axis=0, concat_axis=0, tiled=True)
    pieces = in_order(pieces.reshape(*sizes, *inside), concats[0] + 1)
    return in_order(pieces, concats[1])


def layer_norm(source, gain):
    values = source.astype(jnp.float32)
    center = values - jnp.mean(values, axis=-1, keepdims=True)
    inverse = lax.rsqrt(jnp.mean(center * center, axis=-1, keepdims=True) + epsilon)
    return (center * inverse * gain).astype(jnp.bfloat16)


def stored(product):
    return lax.optimization_barrier(product.astype(jnp.bfloat16)).astype(jnp.float32)


def gla_blocks(queries, key_rows, value_rows, log_decay, state_init):
    length, heads_here, key_width = queries.shape
    value_width = value_rows.shape[-1]
    blocks = length // BLOCK
    query_blocks = queries.reshape(blocks, BLOCK, heads_here, key_width)
    key_blocks = key_rows.reshape(blocks, BLOCK, heads_here, key_width)
    value_blocks = value_rows.reshape(blocks, BLOCK, heads_here, value_width)
    within = jnp.cumsum(log_decay.reshape(blocks, BLOCK, heads_here, key_width), axis=1)
    block_total = within[:, -1]
    scaled_query = query_blocks * jnp.exp(within)
    scaled_key = key_blocks * jnp.exp(-within)
    causal = jnp.tril(jnp.ones((BLOCK, BLOCK), dtype=jnp.bool_))
    scores = jnp.einsum("nihd,njhd->nhij", scaled_query, scaled_key, precision=highest)
    scores = jnp.where(causal, scores, 0.0)
    inside = jnp.einsum("nhij,njhv->nihv", scores, value_blocks, precision=highest)
    block_added = jnp.einsum(
        "njhd,njhv->nhdv",
        key_blocks * jnp.exp(block_total[:, None] - within),
        value_blocks,
        precision=highest,
    )

    def advance(state, inputs):
        decay_sum, addition = inputs
        return (jnp.exp(decay_sum)[:, :, None] * state + addition, state)

    final_state, entering = lax.scan(advance, state_init, (block_total, block_added))
    inside = inside + jnp.einsum("nihd,nhdv->nihv", scaled_query, entering, precision=highest)
    before = jnp.cumsum(block_total, axis=0) - block_total
    carried_query = query_blocks * jnp.exp(within + before[:, None])
    return (
        inside.reshape(length, heads_here, value_width),
        final_state,
        carried_query.reshape(length, heads_here, key_width),
        jnp.sum(block_total, axis=0),
    )


def body(
    mix_rows,
    expert_rows,
    mix_gain,
    ffn_gain,
    w_query,
    w_key,
    w_value,
    w_lowrank,
    w_decay,
    decay_bias,
    decay_shift,
    head_gain,
    w_output,
    route_ids,
    route_weights,
    w_gate,
    w_lift,
    w_drop,
    shared_gate,
    shared_lift,
    shared_drop,
):
    mix_normed = layer_norm(mix_rows, mix_gain)
    local_heads = w_query.shape[1] // DK
    key_cols = local_heads * DK
    value_cols = w_value.shape[1]
    column = lax.axis_index("tp") * key_cols
    decay_cols = lax.dynamic_slice_in_dim(w_decay, column, key_cols, 1)
    bias_cols = lax.dynamic_slice_in_dim(decay_bias, column, key_cols, 0)
    shard_rows = lax.all_gather(mix_normed, "tp", axis=0, tiled=True)
    query_part = jnp.dot(shard_rows, w_query, preferred_element_type=jnp.float32)
    key_part = jnp.dot(shard_rows, w_key, preferred_element_type=jnp.float32)
    value_part = jnp.dot(shard_rows, w_value, preferred_element_type=jnp.float32)
    lowrank = jnp.dot(shard_rows, w_lowrank, preferred_element_type=jnp.float32).astype(
        jnp.bfloat16
    )
    logits = jnp.dot(lowrank, decay_cols, preferred_element_type=jnp.float32) + bias_cols
    projected = jnp.concatenate(
        [stored(query_part), stored(key_part), stored(value_part), logits], axis=1
    )
    span_rows = projected.shape[0]
    queries = projected[:, :key_cols].reshape(span_rows, local_heads, DK) * DK ** (-0.5)
    key_rows = projected[:, key_cols : 2 * key_cols].reshape(span_rows, local_heads, DK)
    value_rows = projected[:, 2 * key_cols : 2 * key_cols + value_cols].reshape(
        span_rows, local_heads, DV
    )
    log_decay = (
        jax.nn.log_sigmoid(projected[:, 2 * key_cols + value_cols :]).reshape(
            span_rows, local_heads, DK
        )
        / gate_norm
        + jnp.transpose(decay_shift)[:, :, None]
    )
    zero_state = jnp.zeros((local_heads, DK, DV), jnp.float32)
    inside, final_state, carried_query, decay_total = gla_blocks(
        queries, key_rows, value_rows, log_decay, zero_state
    )

    def chain(earlier, later):
        return (earlier[0] + later[0], jnp.exp(later[0])[:, :, None] * earlier[1] + later[1])

    carried = carried_in(
        (decay_total, final_state), EP, chain, (jnp.zeros_like(decay_total), zero_state)
    )
    entering = carried[1]
    attended = inside + jnp.einsum("rhd,hdv->rhv", carried_query, entering, precision=highest)
    inverse = lax.rsqrt(jnp.mean(attended * attended, axis=-1, keepdims=True) + epsilon)
    head_rows = (
        (attended * inverse * head_gain).astype(jnp.bfloat16).reshape(span_rows, local_heads * DV)
    )
    mixed = lax.psum_scatter(
        jnp.dot(head_rows, w_output, preferred_element_type=jnp.float32).astype(jnp.bfloat16),
        "tp",
        scatter_dimension=0,
        tiled=True,
    )
    expert_normed = layer_norm(expert_rows, ffn_gain)
    shard_rows = lax.all_gather(expert_normed, "tp", axis=0, tiled=True)
    hidden = (
        jax.nn.silu(jnp.dot(shard_rows, shared_gate, preferred_element_type=jnp.float32))
        * jnp.dot(shard_rows, shared_lift, preferred_element_type=jnp.float32)
    ).astype(jnp.bfloat16)
    shared_sum = lax.psum_scatter(
        jnp.dot(hidden, shared_drop, preferred_element_type=jnp.float32).astype(jnp.bfloat16),
        "tp",
        scatter_dimension=0,
        tiled=True,
    ).astype(jnp.float32)
    own_tokens, top_count = route_ids.shape
    local_experts = w_gate.shape[0]
    experts = lax.axis_size(EP) * lax.axis_size("tp") * local_experts
    capacity = 2 * own_tokens * top_count // experts
    flat_routes = route_ids.reshape(-1)
    matches = (flat_routes[:, None] == jnp.arange(experts, dtype=jnp.int32)[None, :]).astype(
        jnp.int32
    )
    slot_rank = jnp.sum((jnp.cumsum(matches, axis=0) - 1) * matches, axis=1)
    slot_index = flat_routes * capacity + slot_rank
    token_index = jnp.arange(own_tokens * top_count, dtype=jnp.int32) // top_count
    slot_token = (
        jnp.full((experts * capacity,), own_tokens, jnp.int32).at[slot_index].set(token_index)
    )
    padded = jnp.concatenate(
        [expert_normed, jnp.zeros((1, expert_normed.shape[1]), jnp.bfloat16)], axis=0
    )
    outgoing = padded[slot_token].reshape(experts, capacity, -1)
    sectioned = outgoing.reshape(
        lax.axis_size(EP), lax.axis_size("tp"), local_experts, capacity, -1
    )
    arrived = joined_exchange(sectioned, EP_TP, (EP, "tp"), (0, 1), (0, 1))
    arrived_shape = arrived.shape
    grouped = arrived.reshape(-1, local_experts, arrived_shape[-2], arrived_shape[-1])
    gate_part = jnp.einsum("sepd,edf->sepf", grouped, w_gate, preferred_element_type=jnp.float32)
    lift_part = jnp.einsum("sepd,edf->sepf", grouped, w_lift, preferred_element_type=jnp.float32)
    inner = (jax.nn.silu(gate_part) * lift_part).astype(jnp.bfloat16)
    result = jnp.einsum("sepf,efd->sepd", inner, w_drop, preferred_element_type=jnp.float32)
    returned = joined_exchange(
        result.astype(jnp.bfloat16).reshape(arrived_shape), EP_TP, (EP, "tp"), (0, 1), (0, 1)
    )
    results = returned.reshape(experts * capacity, -1)[slot_index].reshape(
        own_tokens, top_count, -1
    )
    combined = shared_sum + jnp.sum(route_weights[:, :, None] * results.astype(jnp.float32), axis=1)
    return (mixed, combined.astype(jnp.bfloat16))


def solution(mesh):
    finer = Mesh(
        mesh.devices.reshape(mesh.shape["grp"], 16, 2, mesh.shape["tp"]),
        ("grp", "ep_0", "ep_1", "tp"),
    )
    in_specs = (
        P(GRP_EP_TP, None),
        P(GRP_EP_TP, None),
        P(),
        P(),
        P(None, "tp"),
        P(None, "tp"),
        P(None, "tp"),
        P(),
        P(),
        P(),
        P("tp", GRP_EP),
        P(),
        P("tp", None),
        P(GRP_EP_TP, None),
        P(GRP_EP_TP, None),
        P(EP_TP, None, None),
        P(EP_TP, None, None),
        P(EP_TP, None, None),
        P(None, "tp"),
        P(None, "tp"),
        P("tp", None),
    )
    out_specs = (P(GRP_EP_TP, None), P(GRP_EP_TP, None))
    return jax.shard_map(body, mesh=finer, in_specs=in_specs, out_specs=out_specs, check_vma=False)
```

profile of v0, /device:TPU:40, one launch (start us, length us, event | category | flops | bytes accessed | tf_op | source)
XLA Modules:
  0.0 543.7 jit_solution(14457288124230649434)
XLA Ops:
  7.2 0.9 copy.77
  8.4 0.7 broadcast_multiply_fusion
  9.2 0.2 fusion.39
  9.7 0.2 fusion.38
  10.0 2.4 scatter_custom_fusion
  12.5 0.2 convert_reduce_fusion
  12.6 0.3 fusion.22
  12.9 0.4 fusion.24
  13.4 6.0 %gather_fusion = bf16[1024,2048]{1,0:T(8,128)(2,1)} fusion(bf16[129,2048]{1,0:T(8,128)(2,1)S(1)} %concatenate.11, s32[1024]{0:T(1024)S(1)} %fusion.134), kind=kCustom, calls=%fused_computation | custom fusion | bytes 8392704 | tf_op jit(solution)/shard_map/gather | solution.py:241
  19.4 32.4 %all-to-all-start = ((bf16[128,1,1,1,8,2048]{5,4,3,2,1,0:T(8,128)(2,1)}), bf16[128,1,1,1,8,2048]{5,4,3,2,1,0:T(8,128)(2,1)}, u32[]{:S(2)}, u32[]{:S(2)}) async-start(bf16[128,1,1,1,8,2048]{5,4,3,2,1,0:T(8,128)(2,1)} %bitcast.204), calls=%async_computation.2 | async-start | bytes 8388608 | tf_op jit(solution)/shard_map/all_to_all | solution.py:81
  51.9 0.2 convert_reduce_fusion.1
  52.0 0.3 fusion.25
  52.3 1.2 fusion.27
  53.6 0.2 all-gather.9.cloned.1.call-start
  53.8 0.6 all-gather.9.cloned.1.call-update
  54.4 180.6 %all-to-all-done = bf16[128,1,1,1,8,2048]{5,4,3,2,1,0:T(8,128)(2,1)} async-done(((bf16[128,1,1,1,8,2048]{5,4,3,2,1,0:T(8,128)(2,1)}), bf16[128,1,1,1,8,2048]{5,4,3,2,1,0:T(8,128)(2,1)}, u32[]{:S(2)}, u32[]{:S(2)}) %all-to-all-start) | async-done | bytes 4194336 | tf_op jit(solution)/shard_map/all_to_all | solution.py:81
  235.0 7.4 %copy.103 = bf16[32,4,1,1,1,8,2048]{6,1,0,5,4,3,2:T(4,128)(2,1)} copy(bf16[32,4,1,1,1,8,2048]{6,5,1,0,4,3,2:T(8,128)(2,1)} %bitcast.41) | data formatting | bytes 8388608 | tf_op jit(solution)/shard_map/reshape | solution.py:82
  242.4 6.9 %reshape.513 = bf16[128,8,2048]{2,0,1:T(8,128)(2,1)} reshape(bf16[32,4,1,1,8,2048]{5,1,0,4,3,2:T(4,128)(2,1)} %bitcast.205) | data formatting | bytes 8388608 | tf_op jit(solution)/shard_map/reshape.103
  249.3 6.6 %fusion.2 = f32[128,8,512]{2,0,1:T(8,128)} fusion(bf16[128,8,2048]{2,0,1:T(8,128)(2,1)} %reshape.513, bf16[1,2048,512]{2,1,0:T(8,128)(2,1)} %param.39), kind=kOutput, calls=%fused_computation.15 | convolution fusion | flops 2147483648 | bytes 8388608 | tf_op jit(solution)/shard_map/sepd,edf->sepf/dot_general | solution.py:249
  255.9 10.1 %convert_bitcast_fusion = bf16[128,1,1,1,8,2048]{5,0,4,3,2,1:T(8,128)(2,1)} fusion(bf16[1,512,2048]{2,1,0:T(8,128)(2,1)S(1)} %copy-done, f32[128,8,512]{2,0,1:T(8,128)} %fusion.2, bf16[128,8,2048]{2,0,1:T(8,128)(2,1)} %reshape.513, bf16[1,2048,512]{2,1,0:T(8,128)(2,1)} %param.38), kind=kOutput, calls=%fused_computation.9 | convolution fusion | flops 4300210176 | bytes 14680064 | tf_op jit(solution)/shard_map/sepf,efd->sepd/dot_general | solution.py:251
  266.0 6.4 %copy.83 = bf16[128,1,1,1,8,2048]{5,4,3,2,1,0:T(8,128)(2,1)} copy(bf16[128,1,1,1,8,2048]{5,0,4,3,2,1:T(8,128)(2,1)} %convert_bitcast_fusion) | data formatting | bytes 8388608 | tf_op jit(solution)/shard_map/reshape;transpose;transpose;reshape;reshape;reshape | solution.py:80
  272.4 14.8 %all-to-all-start.1 = ((bf16[128,1,1,1,8,2048]{5,4,3,2,1,0:T(8,128)(2,1)}), bf16[128,1,1,1,8,2048]{5,4,3,2,1,0:T(8,128)(2,1)}, u32[]{:S(2)}, u32[]{:S(2)}) async-start(bf16[128,1,1,1,8,2048]{5,4,3,2,1,0:T(8,128)(2,1)} %copy.83), calls=%async_computation.3 | async-start | bytes 8388608 | tf_op jit(solution)/shard_map/all_to_all | solution.py:81
  287.5 0.8 dynamic_slice.15
  288.4 2.8 fusion.37
  291.2 0.3 div.46
  291.5 0.4 fusion.33
  292.0 1.9 convolution_convert_fusion.4
  293.9 1.1 mul.314
  295.0 1.7 convolution_convert_fusion.3
  296.8 1.1 reshape.520
  297.9 2.0 convolution_convert_fusion.2
  300.0 2.5 fusion.186
  302.5 4.9 convolution_convert_fusion
  307.5 0.6 slice-done
  308.1 0.4 copy-done.8
  308.6 2.6 exponential_multiply_fusion
  311.2 0.6 fusion.30
  311.8 6.1 %while.13 = (s32[]{:T(128)}, f32[2,64,128]{2,1,0:T(8,128)S(1)}, f32[8,2,64,128]{3,2,1,0:T(8,128)}, f32[8,2,64]{2,0,1:T(8,128)S(1)}, f32[8,2,64,128]{3,2,1,0:T(8,128)S(1)}, /*index=5*/s32[]{:T(128)}, s32[]{:T(128)}) while((s32[]{:T(128)}, f32[2,64,128]{2,1,0:T(8,128)S(1)}, f32[8,2,64,128]{3,2,1,0:T(8,128)}, ...), condition=%wide.region_4.5_spmd.clone, body=%wide.region_3.4_spmd.clone.sunk | while | flops 65539 | bytes 330848 | solution.py:123
  311.8 0.6 bitcast_dynamic-update-slice_fusion.2
  312.6 0.6 bitcast_dynamic-update-slice_fusion.2
  313.3 0.6 bitcast_dynamic-update-slice_fusion.2
  314.1 0.6 bitcast_dynamic-update-slice_fusion.2
  314.9 0.6 bitcast_dynamic-update-slice_fusion.2
  315.6 0.6 bitcast_dynamic-update-slice_fusion.2
  316.4 0.6 bitcast_dynamic-update-slice_fusion.2
  317.2 0.6 bitcast_dynamic-update-slice_fusion.2
  317.9 0.1 copy.72
  318.2 2.0 all-gather.2
  320.3 172.6 %all-gather.3 = bf16[16,129,128]{2,1,0:T(8,128)(2,1)S(1)} all-gather(bf16[1,129,128]{2,1,0:T(8,128)(2,1)S(1)} %maximum_bitcast_fusion.1), channel_id=3, replica_groups=mesh['grp'=2,'ep_0'=16,'ep_1'=2,'tp'=4] {'ep_0'}, dimensions={0}, use_global_device_ids=true | all-gather | bytes 561408 | tf_op jit(solution)/shard_map/all_gather | solution.py:35
  494.5 1.1 convolution_select_fusion
  495.6 0.4 fusion.49
  496.1 0.7 fusion.18
  496.8 0.2 copy.74
  497.0 0.1 copy-done.10
  497.1 0.3 copy.73
  497.4 0.1 exp.273
  497.6 1.5 multiply_reduce_fusion.1
  499.2 2.0 convolution_convert_fusion.1
  501.3 0.6 copy-done.17
  502.1 7.1 %gather_fusion.1 = bf16[512,2048]{1,0:T(8,128)(2,1)S(1)} fusion(bf16[1024,2048]{1,0:T(8,128)(2,1)} %bitcast.68, s32[1024]{0:T(1024)S(1)} %pad_clamp_fusion), kind=kCustom, calls=%fused_computation.1 | custom fusion | bytes 4196352 | tf_op jit(solution)/shard_map/gather | solution.py:255
  509.2 3.0 reshape.541
  512.2 5.5 %multiply_reduce_fusion = f32[128,2048]{1,0:T(8,128)S(1)} fusion(f32[128,4,2048]{2,1,0:T(4,128)} %reshape.541, f32[128,4]{1,0:T(8,128)S(1)} %copy.75), kind=kLoop, calls=%fused_computation.8 | loop fusion | flops 1835008 | bytes 5244928 | tf_op jit(solution)/shard_map/reduce_sum | solution.py:258
  517.8 1.9 add_convert_fusion
  519.7 17.0 %reduce-scatter.3.cloned.1.call-done = bf16[128,2048]{1,0:T(8,128)(2,1)} async-done(((bf16[512,2048]{1,0:T(8,128)(2,1)}), bf16[128,2048]{1,0:T(8,128)(2,1)}) %reduce-scatter.3.cloned.1.call-update) | async-done | bytes 524304 | tf_op jit(solution)/shard_map/reduce_scatter | solution.py:206
  (132 shorter events, 4.7 us)
Async XLA Ops:
  7.2 248.7 %copy-start = (bf16[1,512,2048]{2,1,0:T(8,128)(2,1)S(1)}, bf16[1,512,2048]{2,1,0:T(8,128)(2,1)}, u32[]{:S(2)}) copy-start(bf16[1,512,2048]{2,1,0:T(8,128)(2,1)} %param.40) | copy-start | bytes 6291460
  7.2 5.3 copy-start.4
  7.2 5.7 %copy-start.14 = (f32[2048]{0:T(1024)S(1)}, f32[2048]{0:T(1024)}, u32[]{:S(2)}) copy-start(f32[2048]{0:T(1024)} %param.26) | copy-start | bytes 24580
  13.3 6.1 %copy-start.6 = (bf16[128,2048]{1,0:T(8,128)(2,1)}, bf16[128,2048]{1,0:T(8,128)(2,1)S(1)}, u32[]{:S(2)}) copy-start(bf16[128,2048]{1,0:T(8,128)(2,1)S(1)} %fusion.24) | copy-start | bytes 1572868
  19.4 32.5 %copy-start.5 = (bf16[128,2048]{1,0:T(8,128)(2,1)S(1)}, bf16[128,2048]{1,0:T(8,128)(2,1)}, u32[]{:S(2)}) copy-start(bf16[128,2048]{1,0:T(8,128)(2,1)} %param.23) | copy-start | bytes 1572868
  19.4 32.9 %copy-start.15 = (f32[2048]{0:T(1024)S(1)}, f32[2048]{0:T(1024)}, u32[]{:S(2)}) copy-start(f32[2048]{0:T(1024)} %param.25) | copy-start | bytes 24580
  19.4 215.6 %all-to-all-start = ((bf16[128,1,1,1,8,2048]{5,4,3,2,1,0:T(8,128)(2,1)}), bf16[128,1,1,1,8,2048]{5,4,3,2,1,0:T(8,128)(2,1)}, u32[]{:S(2)}, u32[]{:S(2)}) async-start(bf16[128,1,1,1,8,2048]{5,4,3,2,1,0:T(8,128)(2,1)} %bitcast.204), calls=%async_computation.2 | async-start | bytes 8388608 | tf_op jit(solution)/shard_map/all_to_all | solution.py:81
  51.8 236.5 %all-gather.7.cloned.1.call-start = ((), (), s32[]{:S(2)}) async-start(), calls=%async_computation.4 | async-start | bytes 2621440 | tf_op jit(solution)/shard_map/all_gather | solution.py:165
  53.6 246.4 %all-gather.9.cloned.1.call-start = ((), (), s32[]{:S(2)}) async-start(), calls=%async_computation.6 | async-start | bytes 2621440 | tf_op jit(solution)/shard_map/all_gather | solution.py:213
  272.4 14.9 %copy-start.16 = (f32[2,512]{1,0:T(2,128)S(1)}, f32[2,512]{1,0:T(2,128)}, u32[]{:S(2)}) copy-start(f32[2,512]{1,0:T(2,128)} %param.33) | copy-start | bytes 12292
  272.4 15.9 %copy-start.19 = (bf16[2048,32]{0,1:T(8,128)(2,1)S(1)}, bf16[2048,32]{0,1:T(8,128)(2,1)}, u32[]{:S(2)}) copy-start(bf16[2048,32]{0,1:T(8,128)(2,1)} %param.30) | copy-start | bytes 393220
  272.4 229.7 %all-to-all-start.1 = ((bf16[128,1,1,1,8,2048]{5,4,3,2,1,0:T(8,128)(2,1)}), bf16[128,1,1,1,8,2048]{5,4,3,2,1,0:T(8,128)(2,1)}, u32[]{:S(2)}, u32[]{:S(2)}) async-start(bf16[128,1,1,1,8,2048]{5,4,3,2,1,0:T(8,128)(2,1)} %copy.83), calls=%async_computation.3 | async-start | bytes 8388608 | tf_op jit(solution)/shard_map/all_to_all | solution.py:81
  287.2 230.6 %reduce-scatter.5.cloned.1.call-start = ((), (), s32[]{:S(2)}) async-start(), calls=%async_computation.7 | async-start | bytes 2621440 | tf_op jit(solution)/shard_map/reduce_scatter | solution.py:218
  288.3 3.6 copy-start.3
  291.9 4.9 copy-start.7
  297.9 2.1 copy-start.12
  300.0 2.5 copy-start.2
  307.4 0.7 slice-start
  307.4 1.1 copy-start.8
  307.4 1.2 copy-start.9
  307.5 229.3 %reduce-scatter.3.cloned.1.call-start = ((), (), s32[]{:S(2)}) async-start(), calls=%async_computation.5 | async-start | bytes 2621440 | tf_op jit(solution)/shard_map/reduce_scatter | solution.py:206
  318.1 178.0 %copy-start.13 = (f32[8,2,64,128]{3,2,1,0:T(8,128)S(1)}, f32[8,2,64,128]{3,2,1,0:T(8,128)}, u32[]{:S(2)}) copy-start(f32[8,2,64,128]{3,2,1,0:T(8,128)} %get-tuple-element.30) | copy-start | bytes 1572868
  496.0 1.0 copy-start.10
  497.3 1.7 copy-start.18
  497.5 1.7 copy-start.11
  501.2 0.7 copy-start.17
  512.2 24.5 %copy-start.1 = (bf16[1,512,2048]{2,1,0:T(8,128)(2,1)S(1)}, bf16[1,512,2048]{2,1,0:T(8,128)(2,1)}, u32[]{:S(2)}) copy-start(bf16[1,512,2048]{2,1,0:T(8,128)(2,1)} %param.40) | copy-start | bytes 6291460
Sparse Core Ops, SparseCore 0:
  55.0 41.0 all-gather.6
  98.0 44.0 all-gather.8
  307.6 40.8 reduce-scatter.4
  501.4 35.2 reduce-scatter.2
where the time goes:
time: 551 us; the launch traced here: 544 us
  waiting for transfers between devices  198 us (36%)
  blocking collectives  175 us (32%)
  local copies, waits for them, and re-layouts  49 us (9%)
  starting transfers between devices  47.6 us (9%)
  matrix products  38.7 us (7%)
  other arithmetic  20.3 us (4%)
  between operations  14.8 us (3%)
    all_to_all x2, waiting for transfers between devices, joined_exchange(): lax.all_to_all(pieces, axis, split_axis=0, concat_axis=0, tiled=True)  181 us
    all_gather x2, blocking collectives, gathered_once(): both, at, found = (lax.all_gather(jnp.concatenate(lines), axis), 0, {})  175 us
    all_to_all x2, starting transfers between devices, joined_exchange(): lax.all_to_all(pieces, axis, split_axis=0, concat_axis=0, tiled=True)  47.2 us
    reduce_scatter x1, waiting for transfers between devices, body(): lax.psum_scatter(jnp.dot(head_rows, w_output, preferred_element_type=jnp....  17 us
  transfers between devices with their start and end apart: 6, of which 2 were waited for; matrix products, arithmetic and copies ran while one was open for 17% of the time, Pallas kernels for 0%

commit v1 on v0

--- a/solution.py
+++ b/solution.py
@@ -1,6 +1,10 @@
+import functools
+
 import jax
 import jax.numpy as jnp
 from jax import lax
+from jax.experimental import pallas as pl
+from jax.experimental.pallas import tpu as pltpu
 from jax.sharding import Mesh
 from jax.sharding import PartitionSpec as P
 
@@ -59,28 +63,6 @@
             inside = jax.tree.map(lambda new, old: jnp.where(passed, new, old), total, inside)
         before = combine(inside, before)
     return before
-
-
-def cut_along(value, dim, length):
-    before, after = (value.shape[:dim], value.shape[dim + 1 :])
-    return jnp.moveaxis(value.reshape(*before, length, -1, *after), dim, 0)
-
-
-def in_order(pieces, dim):
-    pieces = jnp.moveaxis(pieces, 0, dim)
-    dims = pieces.shape
-    return pieces.reshape(*dims[:dim], dims[dim] * dims[dim + 1], *dims[dim + 2 :])
-
-
-def joined_exchange(value, axis, axes, splits, concats):
-    sizes = [lax.axis_size(a) for a in axes]
-    pieces = cut_along(value, splits[0], sizes[0])
-    pieces = jnp.moveaxis(cut_along(pieces, splits[1] + 1, sizes[1]), 0, 1)
-    inside = pieces.shape[2:]
-    pieces = pieces.reshape(-1, *inside)
-    pieces = lax.all_to_all(pieces, axis, split_axis=0, concat_axis=0, tiled=True)
-    pieces = in_order(pieces.reshape(*sizes, *inside), concats[0] + 1)
-    return in_order(pieces, concats[1])
 
 
 def layer_norm(source, gain):
@@ -130,6 +112,374 @@
         carried_query.reshape(length, heads_here, key_width),
         jnp.sum(block_total, axis=0),
     )
+
+
+MESH = pl.DeviceIdType.MESH
+
+
+def plane_rows(values, width):
+    return jnp.concatenate(
+        [jnp.broadcast_to(values[j : j + 1], (width, values.shape[1])) for j in range(len(values))],
+        axis=0,
+    )
+
+
+def moe_kernel(
+    nz, nc, nx,
+    rows_ref, meta_ref, gate_hbm, lift_hbm, drop_hbm,
+    out_ref,
+    held, metas, picks, outgoing, arrived, results, back, sums, first,
+    gate_ref, lift_ref, drop_ref, hidden, own_sum,
+    ag_send, ag_recv, meta_send, meta_recv, out_send, out_recv, back_send, back_recv,
+    rs_send, rs_recv, load_sem,
+):
+    half = nz // 2
+    peers = nc * nx
+    z = lax.axis_index("ep_0")
+    core = lax.axis_index("ep_1")
+    col = lax.axis_index("tp")
+    me = core * nx + col
+    tokens, width = rows_ref.shape
+    cut = width // 2
+    slots = arrived.shape[1] // peers
+    cap = slots // 2
+    right, left = lax.rem(z + 1, nz), lax.rem(z + nz - 1, nz)
+    beside = (right, left)
+
+    def peer(i):
+        number = lax.rem(me + i, peers)
+        return number, {"ep_1": number // nx, "tp": lax.rem(number, nx)}
+
+    barrier = pltpu.get_barrier_semaphore()
+    for neighbour in beside:
+        pl.semaphore_signal(barrier, inc=1, device_id={"ep_0": neighbour}, device_id_type=MESH)
+    for i in range(1, peers):
+        pl.semaphore_signal(barrier, inc=1, device_id=peer(i)[1], device_id_type=MESH)
+    loads = [
+        pltpu.make_async_copy(a, b, load_sem.at[k])
+        for k, (a, b) in enumerate(
+            ((gate_hbm, gate_ref), (lift_hbm, lift_ref), (drop_hbm, drop_ref))
+        )
+    ]
+    for load in loads:
+        load.start()
+    held[0, 0:tokens] = rows_ref[...]
+    metas[0, 0:8] = meta_ref[...]
+    pl.semaphore_wait(barrier, peers + 1)
+
+    def place(k, way):
+        if isinstance(k, int) and k == half:
+            return 0, slice(tokens, 2 * tokens)
+        return k, slice(0, tokens) if way == 0 else slice(tokens, 2 * tokens)
+
+    def columns(c):
+        return slice(c * cut, (c + 1) * cut)
+
+    def gather_copy(k, way, c):
+        if isinstance(k, int) and k == 1:
+            source = rows_ref.at[:, columns(c)]
+        else:
+            at, span = place(k - 1, way)
+            source = held.at[at, span, columns(c)]
+        at, span = place(k, way)
+        return pltpu.make_async_remote_copy(
+            source, held.at[at, span, columns(c)],
+            ag_send.at[way, k, c], ag_recv.at[way, k, c],
+            device_id={"ep_0": beside[way]}, device_id_type=MESH,
+        )
+
+    def meta_place(k, way):
+        if isinstance(k, int) and k == half:
+            return 0, slice(8, 16)
+        return k, slice(0, 8) if way == 0 else slice(8, 16)
+
+    def meta_copy(k, way):
+        if isinstance(k, int) and k == 1:
+            source = meta_ref
+        else:
+            at, span = meta_place(k - 1, way)
+            source = metas.at[at, span]
+        at, span = meta_place(k, way)
+        return pltpu.make_async_remote_copy(
+            source, metas.at[at, span], meta_send.at[way, k], meta_recv.at[way, k],
+            device_id={"ep_0": beside[way]}, device_id_type=MESH,
+        )
+
+    def block(number):
+        return pl.ds(pl.multiple_of(number * slots, slots), slots)
+
+    def out_copy(k, i):
+        number, there = peer(i)
+        return pltpu.make_async_remote_copy(
+            outgoing.at[k, block(number)], arrived.at[k, block(me)],
+            out_send.at[k, i], out_recv.at[k, i], device_id=there, device_id_type=MESH,
+        )
+
+    def out_landed(k, i):
+        number, there = peer(peers - i)
+        return pltpu.make_async_remote_copy(
+            outgoing.at[k, block(number)], arrived.at[k, block(number)],
+            out_send.at[k, i], out_recv.at[k, i], device_id=there, device_id_type=MESH,
+        )
+
+    def back_copy(k, i):
+        number, there = peer(i)
+        return pltpu.make_async_remote_copy(
+            results.at[k, block(number)], back.at[k, block(me)],
+            back_send.at[k, i], back_recv.at[k, i], device_id=there, device_id_type=MESH,
+        )
+
+    def back_landed(k, i):
+        number, there = peer(peers - i)
+        return pltpu.make_async_remote_copy(
+            results.at[k, block(number)], back.at[k, block(number)],
+            back_send.at[k, i], back_recv.at[k, i], device_id=there, device_id_type=MESH,
+        )
+
+    experts = (z * peers + lax.broadcasted_iota(jnp.int32, (peers, tokens), 0)).astype(jnp.float32)
+    earlier = (
+        lax.broadcasted_iota(jnp.int32, (tokens, tokens), 0)
+        < lax.broadcasted_iota(jnp.int32, (tokens, tokens), 1)
+    ).astype(jnp.bfloat16)
+    line = lax.broadcasted_iota(jnp.int32, (peers * slots, tokens), 0)
+    slot_of = lax.rem(line, cap).astype(jnp.float32)
+    side_of = lax.rem(line // cap, 2)
+
+    def dispatch(k):
+        meta = metas[k]
+        chosen, weighted = [], []
+        for side in range(2):
+            hits = jnp.zeros((peers, tokens), jnp.float32)
+            weights = jnp.zeros((peers, tokens), jnp.float32)
+            for choice in range(4):
+                row = meta[side * 8 + choice : side * 8 + choice + 1]
+                weight = meta[side * 8 + 4 + choice : side * 8 + 5 + choice]
+                hit = jnp.where(row == experts, 1.0, 0.0)
+                hits = hits + hit
+                weights = weights + hit * weight
+            rank = jnp.dot(
+                hits.astype(jnp.bfloat16), earlier, preferred_element_type=jnp.float32
+            )
+            rank = jnp.where(hits > 0.5, rank, -1.0)
+            match = (plane_rows(rank, slots) == slot_of) & (side_of == side)
+            chosen.append(jnp.where(match, 1.0, 0.0))
+            weighted.append(jnp.where(match, plane_rows(weights, slots), 0.0))
+        picks[k] = jnp.concatenate(weighted, axis=1).astype(jnp.bfloat16)
+        choose = jnp.concatenate(chosen, axis=1).astype(jnp.bfloat16)
+        tile = 512
+
+        @pl.loop(0, width // tile)
+        def _(n):
+            span = pl.ds(pl.multiple_of(n * tile, tile), tile)
+            outgoing[k, :, span] = jnp.dot(
+                choose, held[k, :, span], preferred_element_type=jnp.float32
+            ).astype(jnp.bfloat16)
+
+        for i in range(1, peers):
+            out_copy(k, i).start()
+        arrived[k, block(me)] = outgoing[k, block(me)]
+
+    def experts_on(k):
+        for i in range(1, peers):
+            out_landed(k, i).wait_recv()
+        tile = 256
+
+        @pl.loop(0, hidden.shape[1] // tile)
+        def _(n):
+            span = pl.ds(pl.multiple_of(n * tile, tile), tile)
+            gate = jnp.dot(arrived[k], gate_ref[:, span], preferred_element_type=jnp.float32)
+            lift = jnp.dot(arrived[k], lift_ref[:, span], preferred_element_type=jnp.float32)
+            hidden[:, span] = (gate / (1.0 + jnp.exp(-gate)) * lift).astype(jnp.bfloat16)
+
+        @pl.loop(0, width // tile)
+        def _(n):
+            span = pl.ds(pl.multiple_of(n * tile, tile), tile)
+            results[k, :, span] = jnp.dot(
+                hidden[...], drop_ref[:, span], preferred_element_type=jnp.float32
+            ).astype(jnp.bfloat16)
+
+        for i in range(1, peers):
+            back_copy(k, i).start()
+        back[k, block(me)] = results[k, block(me)]
+
+    for c in range(2):
+        for way in range(2):
+            gather_copy(1, way, c).start()
+    for way in range(2):
+        meta_copy(1, way).start()
+
+    def step(k):
+        for c in range(2):
+            for way in range(2):
+                gather_copy(k, way, c).wait_recv()
+                gather_copy(k + 1, way, c).start()
+        for way in range(2):
+            meta_copy(k, way).wait_recv()
+            meta_copy(k + 1, way).start()
+        dispatch(k)
+
+    for c in range(2):
+        for way in range(2):
+            gather_copy(1, way, c).wait_recv()
+            gather_copy(2, way, c).start()
+    for way in range(2):
+        meta_copy(1, way).wait_recv()
+        meta_copy(2, way).start()
+    dispatch(1)
+    for load in loads:
+        load.wait()
+
+    @pl.loop(2, half - 1)
+    def _(k):
+        step(k)
+        experts_on(k - 1)
+
+    last = half - 1
+    for c in range(2):
+        for way in range(2):
+            gather_copy(last, way, c).wait_recv()
+            if way == c:
+                gather_copy(half, way, c).start()
+    for way in range(2):
+        meta_copy(last, way).wait_recv()
+    meta_copy(half, 0).start()
+    dispatch(last)
+    experts_on(last - 1)
+    for c in range(2):
+        gather_copy(half, c, c).wait_recv()
+    meta_copy(half, 0).wait_recv()
+    dispatch(0)
+    experts_on(last)
+    experts_on(0)
+
+    def combined(k, span):
+        return lax.dot_general(
+            picks[k], back[k, :, span], (((0,), (0,)), ((), ())),
+            preferred_element_type=jnp.float32,
+        )
+
+    def returned(k):
+        for i in range(1, peers):
+            back_landed(k, i).wait_recv()
+
+    def sum_copy(k, way, c):
+        if isinstance(k, int) and k == half:
+            source = first.at[:, columns(c)]
+        else:
+            source = sums.at[way, k, :, columns(c)]
+        return pltpu.make_async_remote_copy(
+            source, sums.at[way, k - 1, :, columns(c)],
+            rs_send.at[way, k, c], rs_recv.at[way, k, c],
+            device_id={"ep_0": beside[way]}, device_id_type=MESH,
+        )
+
+    returned(0)
+    for c in range(2):
+        both = combined(0, columns(c))
+        own_sum[:, columns(c)] = both[0:tokens]
+        first[:, columns(c)] = both[tokens:].astype(jnp.bfloat16)
+        sum_copy(half, c, c).start()
+
+    def pass_on(k, c, landed):
+        both = combined(k, columns(c))
+        for way in range(2):
+            part = both[tokens:] if way == 0 else both[0:tokens]
+            if landed(way, c):
+                sum_copy(k + 1, way, c).wait_recv()
+                part = part + sums[way, k, :, columns(c)].astype(jnp.float32)
+            sums[way, k, :, columns(c)] = part.astype(jnp.bfloat16)
+            sum_copy(k, way, c).start()
+
+    returned(last)
+    for c in range(2):
+        pass_on(last, c, lambda way, c: way == c)
+
+    @pl.loop(1, last)
+    def _(n):
+        k = last - n
+        returned(k)
+        for c in range(2):
+            pass_on(k, c, lambda way, c: True)
+
+    for c in range(2):
+        total = own_sum[:, columns(c)]
+        for way in range(2):
+            sum_copy(1, way, c).wait_recv()
+            total = total + sums[way, 0, :, columns(c)].astype(jnp.float32)
+        out_ref[:, columns(c)] = total
+
+    for c in range(2):
+        for way in range(2):
+            gather_copy(1, way, c).wait_send()
+            sum_copy(1, way, c).wait_send()
+            if way == c:
+                gather_copy(half, way, c).wait_send()
+                sum_copy(half, way, c).wait_send()
+    for way in range(2):
+        meta_copy(1, way).wait_send()
+    meta_copy(half, 0).wait_send()
+
+    @pl.loop(2, half)
+    def _(k):
+        for way in range(2):
+            for c in range(2):
+                gather_copy(k, way, c).wait_send()
+                sum_copy(k, way, c).wait_send()
+            meta_copy(k, way).wait_send()
+
+    @pl.loop(0, half)
+    def _(k):
+        for i in range(1, peers):
+            out_copy(k, i).wait_send()
+            back_copy(k, i).wait_send()
+
+
+def routed(mesh_sizes, rows, ids, weights, w_gate, w_lift, w_drop):
+    nz, nc, nx = mesh_sizes
+    half, peers = nz // 2, nc * nx
+    tokens, width = rows.shape
+    ff = w_gate.shape[-1]
+    cap = 2 * tokens * ids.shape[1] // (nz * peers)
+    slots = 2 * cap
+    meta = jnp.concatenate([ids.T.astype(jnp.float32), weights.T], axis=0)
+    vmem, dma = pltpu.VMEM, pltpu.SemaphoreType.DMA
+    bf = jnp.bfloat16
+    whole = pl.BlockSpec(memory_space=pltpu.VMEM)
+    anywhere = pl.BlockSpec(memory_space=pl.ANY)
+    return pl.pallas_call(
+        functools.partial(moe_kernel, nz, nc, nx),
+        out_shape=jax.ShapeDtypeStruct((tokens, width), jnp.float32),
+        in_specs=[whole, whole, anywhere, anywhere, anywhere],
+        out_specs=whole,
+        scratch_shapes=[
+            vmem((half, 2 * tokens, width), bf),
+            vmem((half, 16, tokens), jnp.float32),
+            vmem((half, peers * slots, 2 * tokens), bf),
+            vmem((half, peers * slots, width), bf),
+            vmem((half, peers * slots, width), bf),
+            vmem((half, peers * slots, width), bf),
+            vmem((half, peers * slots, width), bf),
+            vmem((2, half, tokens, width), bf),
+            vmem((tokens, width), bf),
+            vmem((width, ff), bf),
+            vmem((width, ff), bf),
+            vmem((ff, width), bf),
+            vmem((peers * slots, ff), bf),
+            vmem((tokens, width), jnp.float32),
+            dma((2, half + 1, 2)), dma((2, half + 1, 2)),
+            dma((2, half + 1)), dma((2, half + 1)),
+            dma((half, peers)), dma((half, peers)),
+            dma((half, peers)), dma((half, peers)),
+            dma((2, half + 1, 2)), dma((2, half + 1, 2)),
+            dma((3,)),
+        ],
+        compiler_params=pltpu.CompilerParams(
+            collective_id=0, has_side_effects=True, vmem_limit_bytes=58 * 1024 * 1024
+        ),
+        cost_estimate=pl.CostEstimate(
+            flops=200_000_000_000, bytes_accessed=16 * 2**20, transcendentals=0
+        ),
+    )(rows, meta, w_gate[0], w_lift[0], w_drop[0])
 
 
 def body(
@@ -221,41 +571,10 @@
         scatter_dimension=0,
         tiled=True,
     ).astype(jnp.float32)
-    own_tokens, top_count = route_ids.shape
-    local_experts = w_gate.shape[0]
-    experts = lax.axis_size(EP) * lax.axis_size("tp") * local_experts
-    capacity = 2 * own_tokens * top_count // experts
-    flat_routes = route_ids.reshape(-1)
-    matches = (flat_routes[:, None] == jnp.arange(experts, dtype=jnp.int32)[None, :]).astype(
-        jnp.int32
-    )
-    slot_rank = jnp.sum((jnp.cumsum(matches, axis=0) - 1) * matches, axis=1)
-    slot_index = flat_routes * capacity + slot_rank
-    token_index = jnp.arange(own_tokens * top_count, dtype=jnp.int32) // top_count
-    slot_token = (
-        jnp.full((experts * capacity,), own_tokens, jnp.int32).at[slot_index].set(token_index)
-    )
-    padded = jnp.concatenate(
-        [expert_normed, jnp.zeros((1, expert_normed.shape[1]), jnp.bfloat16)], axis=0
-    )
-    outgoing = padded[slot_token].reshape(experts, capacity, -1)
-    sectioned = outgoing.reshape(
-        lax.axis_size(EP), lax.axis_size("tp"), local_experts, capacity, -1
-    )
-    arrived = joined_exchange(sectioned, EP_TP, (EP, "tp"), (0, 1), (0, 1))
-    arrived_shape = arrived.shape
-    grouped = arrived.reshape(-1, local_experts, arrived_shape[-2], arrived_shape[-1])
-    gate_part = jnp.einsum("sepd,edf->sepf", grouped, w_gate, preferred_element_type=jnp.float32)
-    lift_part = jnp.einsum("sepd,edf->sepf", grouped, w_lift, preferred_element_type=jnp.float32)
-    inner = (jax.nn.silu(gate_part) * lift_part).astype(jnp.bfloat16)
-    result = jnp.einsum("sepf,efd->sepd", inner, w_drop, preferred_element_type=jnp.float32)
-    returned = joined_exchange(
-        result.astype(jnp.bfloat16).reshape(arrived_shape), EP_TP, (EP, "tp"), (0, 1), (0, 1)
-    )
-    results = returned.reshape(experts * capacity, -1)[slot_index].reshape(
-        own_tokens, top_count, -1
-    )
-    combined = shared_sum + jnp.sum(route_weights[:, :, None] * results.astype(jnp.float32), axis=1)
+    sizes = (lax.axis_size("ep_0"), lax.axis_size("ep_1"), lax.axis_size("tp"))
+    combined = shared_sum + routed(
+        sizes, expert_normed, route_ids, route_weights, w_gate, w_lift, w_drop
+    )
     return (mixed, combined.astype(jnp.bfloat16))
 
 

time: 551 us -> 406 us (0.74); the launches traced: 544 us -> 405 us
  Pallas kernels: 0 us -> 217 us
  blocking collectives: 175 us -> 35.7 us
  waiting for transfers between devices: 198 us -> 78.6 us
  starting transfers between devices: 47.6 us -> 0.44 us
  local copies, waits for them, and re-layouts: 49 us -> 9.92 us
  matrix products: 38.7 us -> 23.5 us
  other arithmetic: 20.3 us -> 26.1 us
    pallas_call x0 -> x1, Pallas kernels: none -> 217 us  [routed(): pl.pallas_call(functools.partial(moe_kernel, nz, nc, nx), out_shape=jax.S...]
    all_to_all x2 -> x0, waiting for transfers between devices: 181 us -> none  [joined_exchange(): lax.all_to_all(pieces, axis, split_axis=0, concat_axis=0, tiled=True)]
    all_gather x2, blocking collectives: 175 us -> 35.7 us  [gathered_once(): both, at, found = (lax.all_gather(jnp.concatenate(lines), axis), 0, {})]
    all_to_all x2 -> x0, starting transfers between devices: 47.2 us -> none  [joined_exchange(): lax.all_to_all(pieces, axis, split_axis=0, concat_axis=0, tiled=True)]
    all_gather x1, waiting for transfers between devices: 0.02 us -> 46.7 us  [body(): shard_rows = lax.all_gather(expert_normed, 'tp', axis=0, tiled=True)]
    all_gather x1, waiting for transfers between devices: 0.02 us -> 31.6 us  [body(): shard_rows = lax.all_gather(mix_normed, 'tp', axis=0, tiled=True)]
    reduce_scatter x1, waiting for transfers between devices: 17 us -> 0.01 us  [body(): lax.psum_scatter(jnp.dot(head_rows, w_output, preferred_element_type=jnp....]
    dot_general x2 -> x0, matrix products: 16.6 us -> none  [the longest x1 10.1 us: body(): jnp.einsum('sepf,efd->sepd', inner, w_drop, preferred_element_type=jnp.fl...]
  transfers between devices with their start and end apart: 6 -> 4, of which waited for: 2 -> 2; matrix products, arithmetic and copies ran while one was open for 17% -> 13% of each run, Pallas kernels for 0% -> 53%
where the time goes in v1:
time: 406 us; the launch traced here: 405 us
  Pallas kernels  217 us (53%)
  waiting for transfers between devices  78.6 us (19%)
  blocking collectives  35.7 us (9%)
  other arithmetic  26.1 us (6%)
  matrix products  23.5 us (6%)
  between operations  14.2 us (3%)
  local copies, waits for them, and re-layouts  9.92 us (2%)
    pallas_call x1, Pallas kernels, routed(): pl.pallas_call(functools.partial(moe_kernel, nz, nc, nx), out_shape=jax.S...  217 us
    all_gather x1, waiting for transfers between devices, body(): shard_rows = lax.all_gather(expert_normed, 'tp', axis=0, tiled=True)  46.7 us
    all_gather x2, blocking collectives, gathered_once(): both, at, found = (lax.all_gather(jnp.concatenate(lines), axis), 0, {})  35.7 us
    all_gather x1, waiting for transfers between devices, body(): shard_rows = lax.all_gather(mix_normed, 'tp', axis=0, tiled=True)  31.6 us
  transfers between devices with their start and end apart: 4, of which 2 were waited for; matrix products, arithmetic and copies ran while one was open for 13% of the time, Pallas kernels for 53%

profile of v1, /device:TPU:40, one launch (start us, length us, event | category | flops | bytes accessed | tf_op | source)
XLA Modules:
  0.0 405.3 jit_solution(2992725585201107059)
XLA Ops:
  7.3 1.3 convert_reduce_fusion
  8.6 1.3 fusion.8
  10.0 2.2 fusion.10.rows_ref
  12.3 0.2 convert_reduce_fusion.1
  12.5 0.3 fusion.11
  12.8 1.2 fusion.13
  14.3 0.1 copy.48
  14.4 0.8 dynamic_slice.15
  15.1 0.6 pad_maximum_fusion.meta_ref
  15.7 46.7 %all-gather.9.cloned.1.call-done = bf16[512,2048]{1,0:T(8,128)(2,1)} async-done(((bf16[128,2048]{1,0:T(8,128)(2,1)}), bf16[512,2048]{1,0:T(8,128)(2,1)}) %all-gather.9.cloned.1.call-update) | async-done | bytes 2097168 | tf_op jit(solution)/shard_map/all_gather | solution.py:563
  62.5 2.5 fusion.159
  65.0 4.9 %convolution_convert_fusion = bf16[512,2048]{1,0:T(8,128)(2,1)} fusion(bf16[128,2048]{1,0:T(8,128)(2,1)} %param.43, bf16[512,2048]{1,0:T(8,128)(2,1)S(1)} %copy-done.2, bf16[2048,128]{1,0:T(8,128)(2,1)} %param.42, f32[512,128]{1,0:T(8,128)S(1)} %fusion.159), kind=kOutput, calls=%fused_computation.4 | convolution fusion | flops 538312704 | bytes 5505024 | tf_op jit(solution)/shard_map/dot_general | solution.py:569
  69.9 0.2 reduce-scatter.3.cloned.1.call-start
  70.2 31.6 %all-gather.7.cloned.1.call-done = bf16[512,2048]{1,0:T(8,128)(2,1)} async-done(((bf16[128,2048]{1,0:T(8,128)(2,1)}), bf16[512,2048]{1,0:T(8,128)(2,1)}) %all-gather.7.cloned.1.call-update) | async-done | bytes 2097168 | tf_op jit(solution)/shard_map/all_gather | solution.py:515
  101.8 3.2 convolution_convert_fusion.3
  105.0 1.8 convolution_convert_fusion.4
  106.8 0.7 convert_multiply_fusion
  107.6 1.4 convolution_convert_fusion.2
  109.0 1.0 reshape_reshape.13
  110.0 2.7 fusion.21
  112.7 1.3 div.34
  114.0 0.4 fusion.17
  114.5 1.1 mul.280
  115.6 1.1 reshape.424
  116.7 2.7 exponential_multiply_fusion
  119.5 1.4 fusion.14
  120.9 12.9 %while.13 = (s32[]{:T(128)}, f32[2,64,128]{2,1,0:T(8,128)S(1)}, f32[8,2,64,128]{3,2,1,0:T(8,128)}, f32[8,2,64]{2,0,1:T(8,128)S(1)}, f32[8,2,64,128]{3,2,1,0:T(8,128)}, /*index=5*/s32[]{:T(128)}, s32[]{:T(128)}) while((s32[]{:T(128)}, f32[2,64,128]{2,1,0:T(8,128)S(1)}, f32[8,2,64,128]{3,2,1,0:T(8,128)}, f32[8,2,64]{2,0,1:T(8,128)S(1)}, ...), condition=%wide.region_4.5_spmd.clone, body=%wide.region_3.4_spmd.clone.sunk | while | flops 65539 | bytes 330348 | solution.py:105
  120.9 0.6 bitcast_dynamic-update-slice_fusion.2
  121.5 0.9 bitcast_add_fusion.4
  122.5 0.6 bitcast_dynamic-update-slice_fusion.2
  123.1 0.9 bitcast_add_fusion.4
  124.1 0.6 bitcast_dynamic-update-slice_fusion.2
  124.7 0.9 bitcast_add_fusion.4
  125.7 0.6 bitcast_dynamic-update-slice_fusion.2
  126.4 0.9 bitcast_add_fusion.4
  127.3 0.6 bitcast_dynamic-update-slice_fusion.2
  128.0 0.9 bitcast_add_fusion.4
  128.9 0.6 bitcast_dynamic-update-slice_fusion.2
  129.6 0.9 bitcast_add_fusion.4
  130.6 0.6 bitcast_dynamic-update-slice_fusion.2
  131.2 0.9 bitcast_add_fusion.4
  132.2 0.6 bitcast_dynamic-update-slice_fusion.2
  132.8 0.9 bitcast_add_fusion.4
  133.7 0.1 copy.61
  133.9 0.1 convert_element_type.385
  134.0 1.0 copy.62
  135.0 1.2 exp.269
  136.2 1.1 convolution_select_fusion
  137.3 0.4 fusion.30
  137.7 0.7 fusion.4
  138.4 0.2 copy.63
  138.6 1.9 all-gather.2
  140.6 0.1 exp.232
  140.7 0.1 mul.326
  140.7 0.1 exp.267
  140.8 0.1 fusion.54
  141.0 33.8 %all-gather.3 = bf16[16,129,128]{2,1,0:T(8,128)(2,1)S(1)} all-gather(bf16[1,129,128]{2,1,0:T(8,128)(2,1)S(1)} %maximum_bitcast_fusion.1), channel_id=3, replica_groups=mesh['grp'=2,'ep_0'=16,'ep_1'=2,'tp'=4] {'ep_0'}, dimensions={0}, use_global_device_ids=true | all-gather | bytes 561408 | tf_op jit(solution)/shard_map/all_gather | solution.py:39
  174.8 0.1 exp.237
  174.8 0.1 mul.307
  176.1 1.5 multiply_reduce_fusion
  177.6 0.1 multiply_convert_fusion
  177.7 2.0 convolution_convert_fusion.1
  179.8 216.6 %shard_map.212 = f32[128,2048]{1,0:T(8,128)} custom-call(bf16[128,2048]{1,0:T(8,128)(2,1)} %fusion.10.rows_ref, f32[8,128]{1,0:T(8,128)} %pad_maximum_fusion.meta_ref, bf16[2048,512]{1,0:T(8,128)(2,1)} %bitcast.138, bf16[2048,512]{1,0:T(8,128)(2,1)} %bitcast.139, bf16[512,2048]{1,0:T(8,128)(2,1)} %bitcast.140), custom_call_target="tpu_custom_call" | custom-call | flops 199999995904 | bytes 16777216 | tf_op jit(solution)/shard_map/pallas_call | solution.py:449
  396.5 2.3 add_convert_fusion
  (88 shorter events, 2.1 us)
Async XLA Ops:
  7.2 170.6 %copy-start = (bf16[256,2048]{1,0:T(8,128)(2,1)S(1)}, bf16[256,2048]{1,0:T(8,128)(2,1)}, u32[]{:S(2)}) copy-start(bf16[256,2048]{1,0:T(8,128)(2,1)} %param.35) | copy-start | bytes 3145732
  7.2 5.1 %copy-start.3 = (bf16[128,2048]{1,0:T(8,128)(2,1)S(1)}, bf16[128,2048]{1,0:T(8,128)(2,1)}, u32[]{:S(2)}) copy-start(bf16[128,2048]{1,0:T(8,128)(2,1)} %param.23) | copy-start | bytes 1572868
  7.2 5.6 %copy-start.8 = (f32[2048]{0:T(1024)S(1)}, f32[2048]{0:T(1024)}, u32[]{:S(2)}) copy-start(f32[2048]{0:T(1024)} %param.25) | copy-start | bytes 24580
  7.2 55.3 %all-gather.9.cloned.1.call-start = ((), (), s32[]{:S(2)}) async-start(), calls=%async_computation.4 | async-start | bytes 2621440 | tf_op jit(solution)/shard_map/all_gather | solution.py:563
  9.9 4.2 %copy-start.9 = (f32[2,512]{1,0:T(2,128)S(1)}, f32[2,512]{1,0:T(2,128)}, u32[]{:S(2)}) copy-start(f32[2,512]{1,0:T(2,128)} %param.33) | copy-start | bytes 12292
  9.9 5.2 %copy-start.10 = (s32[128,4]{0,1:T(4,128)S(1)}, s32[128,4]{0,1:T(4,128)}, u32[]{:S(2)}) copy-start(s32[128,4]{0,1:T(4,128)} %param.36) | copy-start | bytes 6148
  9.9 5.2 %copy-start.11 = (f32[128,4]{0,1:T(4,128)S(1)}, f32[128,4]{0,1:T(4,128)}, u32[]{:S(2)}) copy-start(f32[128,4]{0,1:T(4,128)} %param.37) | copy-start | bytes 6148
  12.3 89.5 %all-gather.7.cloned.1.call-start = ((), (), s32[]{:S(2)}) async-start(), calls=%async_computation.2 | async-start | bytes 2621440 | tf_op jit(solution)/shard_map/all_gather | solution.py:515
  14.0 382.4 %reduce-scatter.5.cloned.1.call-start = ((), (), s32[]{:S(2)}) async-start(), calls=%async_computation.5 | async-start | bytes 2621440 | tf_op jit(solution)/shard_map/reduce_scatter | solution.py:568
  62.5 2.5 copy-start.2
  69.9 328.8 %reduce-scatter.3.cloned.1.call-start = ((), (), s32[]{:S(2)}) async-start(), calls=%async_computation.3 | async-start | bytes 2621440 | tf_op jit(solution)/shard_map/reduce_scatter | solution.py:556
  101.8 3.2 copy-start.1
  105.0 2.6 copy-start.13
  112.7 1.8 copy-start.4
  112.7 2.9 copy-start.7
  119.5 14.5 %copy-start.5 = (f32[8,64,2,64]{3,0,1,2:T(8,128)S(1)}, f32[8,64,2,64]{3,0,1,2:T(8,128)}, u32[]{:S(2)}) copy-start(f32[8,64,2,64]{3,0,1,2:T(8,128)} %get-tuple-element.115) | copy-start | bytes 786436
  136.2 1.5 copy-start.6
  140.9 36.7 %copy-start.12 = (f32[128]{0:T(128)S(1)}, f32[128]{0:T(128)}, u32[]{:S(2)}) copy-start(f32[128]{0:T(128)} %param.34) | copy-start | bytes 1540
Sparse Core Ops, SparseCore 0:
  12.4 50.0 all-gather.8
  64.9 36.8 all-gather.6
  104.4 35.8 reduce-scatter.4
  180.0 48.3 reduce-scatter.2

commit v2 on v1

--- a/solution.py
+++ b/solution.py
@@ -22,49 +22,6 @@
 highest = lax.Precision.HIGHEST
 
 
-def filled_with(value, identity):
-    return jax.tree.map(
-        lambda a, e: jnp.broadcast_to(jnp.asarray(e, a.dtype), a.shape), value, identity
-    )
-
-
-def gathered_once(value, axis):
-    leaves = jax.tree.leaves(value)
-    sequence = sorted(range(len(leaves)), key=lambda k: -leaves[k].size)
-    width = (1, *leaves[sequence[0]].shape)[-1]
-    lines = [
-        jnp.pad(leaves[k].reshape(-1), (0, -leaves[k].size % width)).reshape(-1, width)
-        for k in sequence
-    ]
-    both, at, found = (lax.all_gather(jnp.concatenate(lines), axis), 0, {})
-    for k, line in zip(sequence, lines):
-        share = both[:, at : at + len(line)].reshape(len(both), -1)
-        found[k] = share[:, : leaves[k].size].reshape(-1, *leaves[k].shape)
-        at += len(line)
-    numbers = iter(range(len(leaves)))
-    return jax.tree.map(lambda _: found[next(numbers)], value)
-
-
-def carried_in(value, axes, combine, identity):
-    before = start = filled_with(value, identity)
-    total = value
-    for axis in reversed(axes):
-        length, mine = (lax.axis_size(axis), lax.axis_index(axis))
-        pieces = gathered_once(
-            jax.tree.map(lambda part, kind: part.astype(kind), total, (jnp.bfloat16, jnp.bfloat16)),
-            axis,
-        )
-        inside, total = (start, start)
-        for k in range(length):
-            passed = k < mine
-            total = combine(
-                total, jax.tree.map(lambda part, own: part[k].astype(own.dtype), pieces, value)
-            )
-            inside = jax.tree.map(lambda new, old: jnp.where(passed, new, old), total, inside)
-        before = combine(inside, before)
-    return before
-
-
 def layer_norm(source, gain):
     values = source.astype(jnp.float32)
     center = values - jnp.mean(values, axis=-1, keepdims=True)
@@ -72,48 +29,6 @@
     return (center * inverse * gain).astype(jnp.bfloat16)
 
 
-def stored(product):
-    return lax.optimization_barrier(product.astype(jnp.bfloat16)).astype(jnp.float32)
-
-
-def gla_blocks(queries, key_rows, value_rows, log_decay, state_init):
-    length, heads_here, key_width = queries.shape
-    value_width = value_rows.shape[-1]
-    blocks = length // BLOCK
-    query_blocks = queries.reshape(blocks, BLOCK, heads_here, key_width)
-    key_blocks = key_rows.reshape(blocks, BLOCK, heads_here, key_width)
-    value_blocks = value_rows.reshape(blocks, BLOCK, heads_here, value_width)
-    within = jnp.cumsum(log_decay.reshape(blocks, BLOCK, heads_here, key_width), axis=1)
-    block_total = within[:, -1]
-    scaled_query = query_blocks * jnp.exp(within)
-    scaled_key = key_blocks * jnp.exp(-within)
-    causal = jnp.tril(jnp.ones((BLOCK, BLOCK), dtype=jnp.bool_))
-    scores = jnp.einsum("nihd,njhd->nhij", scaled_query, scaled_key, precision=highest)
-    scores = jnp.where(causal, scores, 0.0)
-    inside = jnp.einsum("nhij,njhv->nihv", scores, value_blocks, precision=highest)
-    block_added = jnp.einsum(
-        "njhd,njhv->nhdv",
-        key_blocks * jnp.exp(block_total[:, None] - within),
-        value_blocks,
-        precision=highest,
-    )
-
-    def advance(state, inputs):
-        decay_sum, addition = inputs
-        return (jnp.exp(decay_sum)[:, :, None] * state + addition, state)
-
-    final_state, entering = lax.scan(advance, state_init, (block_total, block_added))
-    inside = inside + jnp.einsum("nihd,nhdv->nihv", scaled_query, entering, precision=highest)
-    before = jnp.cumsum(block_total, axis=0) - block_total
-    carried_query = query_blocks * jnp.exp(within + before[:, None])
-    return (
-        inside.reshape(length, heads_here, value_width),
-        final_state,
-        carried_query.reshape(length, heads_here, key_width),
-        jnp.sum(block_total, axis=0),
-    )
-
-
 MESH = pl.DeviceIdType.MESH
 
 
@@ -126,15 +41,24 @@
 
 def moe_kernel(
     nz, nc, nx,
-    rows_ref, meta_ref, gate_hbm, lift_hbm, drop_hbm,
-    out_ref,
+    mix_ref, rows_ref, meta_ref, shift_ref, decay_ref, bias_ref, gain_ref,
+    gate_hbm, lift_hbm, drop_hbm, query_hbm, key_hbm, value_hbm, low_hbm, mixout_hbm,
+    sgate_hbm, slift_hbm, sdrop_hbm,
+    mixed_ref, out_ref,
     held, metas, picks, outgoing, arrived, results, back, sums, first,
-    gate_ref, lift_ref, drop_ref, hidden, own_sum,
+    gate_ref, lift_ref, drop_ref, query_ref, key_ref, value_ref, low_ref, mixout_ref,
+    sgate_ref, slift_ref, sdrop_ref, hidden, own_sum,
+    mix_all, exp_all, exp_part, mix_sums, exp_sums,
+    q_rows, k_rows, v_rows, decays, inner, carried, state, before,
+    chip_state, chip_total, mate_state, mate_total, prefix, prefix_total,
+    scan_out, scan_total_out, scan_in, scan_total_in, entering,
     ag_send, ag_recv, meta_send, meta_recv, out_send, out_recv, back_send, back_recv,
     rs_send, rs_recv, load_sem,
+    xg_send, xg_recv, xr_send, xr_recv, mate_send, mate_recv, scan_send, scan_recv,
 ):
     half = nz // 2
     peers = nc * nx
+    mix_part = mix_all
     z = lax.axis_index("ep_0")
     core = lax.axis_index("ep_1")
     col = lax.axis_index("tp")
@@ -151,21 +75,29 @@
         return number, {"ep_1": number // nx, "tp": lax.rem(number, nx)}
 
     barrier = pltpu.get_barrier_semaphore()
-    for neighbour in beside:
-        pl.semaphore_signal(barrier, inc=1, device_id={"ep_0": neighbour}, device_id_type=MESH)
+    reaches = [d for d in (1, 2, 4, 8, 16, 32) if d < nz]
+    near = sorted({d % nz for d in reaches} | {-d % nz for d in reaches})
+    for d in near:
+        there = {"ep_0": lax.rem(z + d, nz)}
+        pl.semaphore_signal(barrier, inc=1, device_id=there, device_id_type=MESH)
     for i in range(1, peers):
         pl.semaphore_signal(barrier, inc=1, device_id=peer(i)[1], device_id_type=MESH)
     loads = [
         pltpu.make_async_copy(a, b, load_sem.at[k])
         for k, (a, b) in enumerate(
-            ((gate_hbm, gate_ref), (lift_hbm, lift_ref), (drop_hbm, drop_ref))
+            (
+                (query_hbm, query_ref), (key_hbm, key_ref), (value_hbm, value_ref),
+                (low_hbm, low_ref), (gate_hbm, gate_ref), (lift_hbm, lift_ref),
+                (drop_hbm, drop_ref), (sgate_hbm, sgate_ref), (slift_hbm, slift_ref),
+                (sdrop_hbm, sdrop_ref), (mixout_hbm, mixout_ref),
+            )
         )
     ]
     for load in loads:
         load.start()
     held[0, 0:tokens] = rows_ref[...]
     metas[0, 0:8] = meta_ref[...]
-    pl.semaphore_wait(barrier, peers + 1)
+    pl.semaphore_wait(barrier, peers - 1 + len(near))
 
     def place(k, way):
         if isinstance(k, int) and k == half:
@@ -302,6 +234,279 @@
             back_copy(k, i).start()
         back[k, block(me)] = results[k, block(me)]
 
+    side_cols = (lax.rem(col + 1, nx), lax.rem(col + nx - 1, nx))
+    turn = nx // 2
+
+    def off(k, way):
+        return lax.rem(col + k, nx) if way == 0 else lax.rem(col + nx - k, nx)
+
+    def row_block(number):
+        return pl.ds(pl.multiple_of(number * tokens, tokens), tokens)
+
+    def spread_copy(which, k, way, c, landed=False):
+        source, full = (mix_ref, mix_all) if which == 0 else (rows_ref, exp_all)
+        at = row_block(off(k if landed else k - 1, 1 - way))
+        return pltpu.make_async_remote_copy(
+            source.at[:, columns(c)] if k == 1 else full.at[at, columns(c)],
+            full.at[at, columns(c)],
+            xg_send.at[which, k, way, c], xg_recv.at[which, k, way, c],
+            device_id={"tp": side_cols[way]}, device_id_type=MESH,
+        )
+
+    def spread_start(which):
+        for c in range(2):
+            for way in range(2):
+                spread_copy(which, 1, way, c).start()
+
+    def spread_turn(which):
+        for c in range(2):
+            for way in range(2):
+                spread_copy(which, 1, way, c, True).wait_recv()
+                if way == c:
+                    spread_copy(which, turn, way, c).start()
+
+    def spread_end(which):
+        for c in range(2):
+            spread_copy(which, turn, c, c, True).wait_recv()
+
+    def spread_sent(which):
+        for c in range(2):
+            for way in range(2):
+                spread_copy(which, 1, way, c).wait_send()
+            spread_copy(which, turn, c, c).wait_send()
+
+    def fold_copy(which, k, way, c):
+        part, sums_in = (mix_part, mix_sums) if which == 0 else (exp_part, exp_sums)
+        return pltpu.make_async_remote_copy(
+            part.at[row_block(off(k, way)), columns(c)],
+            sums_in.at[way, k - 1, :, columns(c)],
+            xr_send.at[which, k, way, c], xr_recv.at[which, k, way, c],
+            device_id={"tp": side_cols[way]}, device_id_type=MESH,
+        )
+
+    def fold_start(which):
+        for c in range(2):
+            fold_copy(which, turn, c, c).start()
+            fold_copy(which, 1, 1 - c, c).start()
+
+    def fold_turn(which):
+        part, sums_in = (mix_part, mix_sums) if which == 0 else (exp_part, exp_sums)
+        for c in range(2):
+            fold_copy(which, turn, c, c).wait_recv()
+            at = row_block(off(1, c))
+            part[at, columns(c)] = (
+                part[at, columns(c)].astype(jnp.float32)
+                + sums_in[c, 1, :, columns(c)].astype(jnp.float32)
+            ).astype(jnp.bfloat16)
+            fold_copy(which, 1, c, c).start()
+
+    def fold_end(which, c):
+        part, sums_in = (mix_part, mix_sums) if which == 0 else (exp_part, exp_sums)
+        total = part[row_block(col), columns(c)].astype(jnp.float32)
+        for way in range(2):
+            fold_copy(which, 1, way, c).wait_recv()
+            total = total + sums_in[way, 0, :, columns(c)].astype(jnp.float32)
+        return total
+
+    def fold_sent(which):
+        for c in range(2):
+            for way in range(2):
+                fold_copy(which, 1, way, c).wait_send()
+            fold_copy(which, turn, c, c).wait_send()
+
+    keys = q_rows.shape[1]
+    values = v_rows.shape[1]
+    dv = values // (keys // DK)
+    lane_head = lax.broadcasted_iota(jnp.int32, (1, keys), 1) // DK
+    head_masks = [jnp.where(lane_head == h, 1.0, 0.0) for h in range(2)]
+
+    def project():
+        @pl.loop(0, mix_all.shape[0] // (2 * tokens))
+        def _(n):
+            span = pl.ds(pl.multiple_of(n * 2 * tokens, 2 * tokens), 2 * tokens)
+            rows = mix_all[span]
+            f32 = jnp.float32
+            query = jnp.dot(rows, query_ref[...], preferred_element_type=f32)
+            q_rows[span] = query.astype(jnp.bfloat16)
+            key = jnp.dot(rows, key_ref[...], preferred_element_type=f32)
+            k_rows[span] = key.astype(jnp.bfloat16)
+            value = jnp.dot(rows, value_ref[...], preferred_element_type=f32)
+            v_rows[span] = value.astype(jnp.bfloat16)
+            low = jnp.dot(rows, low_ref[...], preferred_element_type=f32).astype(jnp.bfloat16)
+            logit = jnp.dot(low, decay_ref[...], preferred_element_type=f32) + bias_ref[...]
+            soft = jnp.minimum(logit, 0.0) - jnp.log1p(jnp.exp(-jnp.abs(logit)))
+            decays[span] = soft * (1.0 / gate_norm) + shift_ref[span]
+
+        state[...] = jnp.zeros_like(state)
+        before[...] = jnp.zeros_like(before)
+
+    def scan_blocks(start, stop):
+        low_tri = jnp.where(
+            lax.broadcasted_iota(jnp.int32, (BLOCK, BLOCK), 0)
+            >= lax.broadcasted_iota(jnp.int32, (BLOCK, BLOCK), 1),
+            1.0,
+            0.0,
+        )
+        causal = jnp.concatenate([low_tri, low_tri], axis=0)
+        head_mask = jnp.concatenate(
+            [jnp.broadcast_to(m, (dv, keys)) for m in head_masks], axis=0
+        )
+
+        @pl.loop(start, stop)
+        def _(n):
+            span = pl.ds(pl.multiple_of(n * BLOCK, BLOCK), BLOCK)
+            within = jnp.dot(
+                low_tri, decays[span], precision=highest, preferred_element_type=jnp.float32
+            )
+            total = within[BLOCK - 1 : BLOCK]
+            query = q_rows[span].astype(jnp.float32) * DK ** (-0.5)
+            key = k_rows[span].astype(jnp.float32)
+            value = v_rows[span]
+            scaled = query * jnp.exp(within)
+            scaled_key = (key * jnp.exp(-within)).astype(jnp.bfloat16)
+            kept_key = (key * jnp.exp(total - within)).astype(jnp.bfloat16)
+            both = jnp.concatenate([scaled * m for m in head_masks], axis=0).astype(jnp.bfloat16)
+            scores = lax.dot_general(
+                both, scaled_key, (((1,), (1,)), ((), ())), preferred_element_type=jnp.float32
+            )
+            scores = jnp.where(causal > 0.5, scores, 0.0).astype(jnp.bfloat16)
+            mixed = jnp.dot(scores, value, preferred_element_type=jnp.float32)
+            mixed = jnp.concatenate([mixed[:BLOCK, :dv], mixed[BLOCK:, dv:]], axis=1)
+            mixed = mixed + lax.dot_general(
+                scaled.astype(jnp.bfloat16), state[...].astype(jnp.bfloat16),
+                (((1,), (1,)), ((), ())), preferred_element_type=jnp.float32,
+            )
+            inner[span] = mixed
+            added = lax.dot_general(
+                value, kept_key, (((0,), (0,)), ((), ())), preferred_element_type=jnp.float32
+            )
+            state[...] = jnp.exp(total) * state[...] + added * head_mask
+            carried[span] = (query * jnp.exp(within + before[0:1])).astype(jnp.bfloat16)
+            before[...] = before[...] + total
+
+    mate = {"ep_1": nc - 1 - core}
+
+    def mate_copy(part):
+        source, target = (
+            (chip_state, mate_state), (chip_total, mate_total),
+            (scan_out.at[len(reaches) + 1], entering.at[pl.ds(pl.multiple_of(core * (dv // 2), dv // 2), dv // 2)]),
+        )[part]
+        return pltpu.make_async_remote_copy(
+            source, target, mate_send.at[part], mate_recv.at[part],
+            device_id=mate, device_id_type=MESH,
+        )
+
+    def mate_half_landed():
+        other = nc - 1 - core
+        return pltpu.make_async_remote_copy(
+            scan_out.at[len(reaches) + 1],
+            entering.at[pl.ds(pl.multiple_of(other * (dv // 2), dv // 2), dv // 2)],
+            mate_send.at[2], mate_recv.at[2], device_id=mate, device_id_type=MESH,
+        )
+
+    def states_out():
+        packed = state[0:dv] * head_masks[0] + state[dv:] * head_masks[1]
+        chip_state[...] = packed.astype(jnp.bfloat16)
+        chip_total[...] = before[...]
+        mate_copy(0).start()
+        mate_copy(1).start()
+
+    def scan_copies(step):
+        there = {"ep_0": lax.rem(z + (1 if step == 0 else reaches[step - 1]), nz)}
+        return [
+            pltpu.make_async_remote_copy(
+                a.at[step], b.at[step], scan_send.at[step, n], scan_recv.at[step, n],
+                device_id=there, device_id_type=MESH,
+            )
+            for n, (a, b) in enumerate(
+                ((scan_out, scan_in), (scan_total_out, scan_total_in))
+            )
+        ]
+
+    def scan_start(step):
+        scan_out[step] = prefix[...].astype(jnp.bfloat16)
+        scan_total_out[step] = prefix_total[...]
+        for copy in scan_copies(step):
+            copy.start()
+
+    def scan_open():
+        mate_copy(0).wait_recv()
+        mate_copy(1).wait_recv()
+        early = core == 0
+        own, own_total = chip_state[...].astype(jnp.float32), chip_total[...]
+        far, far_total = mate_state[...].astype(jnp.float32), mate_total[...]
+        later_total = jnp.where(early, far_total[0:1], own_total[0:1])
+        joined = jnp.exp(later_total) * jnp.where(early, own, far) + jnp.where(early, far, own)
+        prefix[...] = jnp.where(early, joined[: dv // 2], joined[dv // 2 :])
+        prefix_total[...] = own_total + far_total
+        scan_start(0)
+
+    def scan_step(step):
+        for copy in scan_copies(step):
+            copy.wait_recv()
+        came = scan_in[step].astype(jnp.float32)
+        came_total = scan_total_in[step]
+        if step == 0:
+            valid = z >= 1
+            prefix[...] = jnp.where(valid, came, 0.0)
+            prefix_total[...] = jnp.where(valid, came_total, 0.0)
+        else:
+            valid = z >= reaches[step - 1]
+            joined = jnp.exp(prefix_total[0:1]) * came + prefix[...]
+            prefix[...] = jnp.where(valid, joined, prefix[...])
+            prefix_total[...] = jnp.where(
+                valid, prefix_total[...] + came_total, prefix_total[...]
+            )
+        if step < len(reaches):
+            scan_start(step + 1)
+        else:
+            mine = prefix[...].astype(jnp.bfloat16)
+            scan_out[step + 1] = mine
+            entering[pl.ds(pl.multiple_of(core * (dv // 2), dv // 2), dv // 2)] = mine
+            mate_copy(2).start()
+
+    def finish_mixer():
+        mate_half_landed().wait_recv()
+        come = entering[...].astype(jnp.float32)
+        behind = jnp.exp(mate_total[0:1]) * come + mate_state[...].astype(jnp.float32)
+        come = jnp.where(core == 0, come, behind)
+        spread_sent(0)
+        wide = jnp.concatenate([come * m for m in head_masks], axis=0).astype(jnp.bfloat16)
+
+        @pl.loop(0, nx)
+        def _(b):
+            span = row_block(b)
+            attended = inner[span] + lax.dot_general(
+                carried[span], wide, (((1,), (1,)), ((), ())), preferred_element_type=jnp.float32
+            )
+            heads = []
+            for h in range(2):
+                one = attended[:, h * dv : (h + 1) * dv]
+                inverse = lax.rsqrt(jnp.mean(one * one, axis=-1, keepdims=True) + epsilon)
+                heads.append((one * inverse * gain_ref[...]).astype(jnp.bfloat16))
+            mix_part[span] = jnp.dot(
+                jnp.concatenate(heads, axis=1), mixout_ref[...], preferred_element_type=jnp.float32
+            ).astype(jnp.bfloat16)
+
+        fold_start(0)
+
+    def shared():
+        @pl.loop(0, nx // 2)
+        def _(n):
+            span = pl.ds(pl.multiple_of(n * 2 * tokens, 2 * tokens), 2 * tokens)
+            rows = exp_all[span]
+            gate = jnp.dot(rows, sgate_ref[...], preferred_element_type=jnp.float32)
+            lift = jnp.dot(rows, slift_ref[...], preferred_element_type=jnp.float32)
+            unit = (gate / (1.0 + jnp.exp(-gate)) * lift).astype(jnp.bfloat16)
+            exp_part[span] = jnp.dot(
+                unit, sdrop_ref[...], preferred_element_type=jnp.float32
+            ).astype(jnp.bfloat16)
+
+        fold_start(1)
+
+    mix_all[row_block(col)] = mix_ref[...]
+    exp_all[row_block(col)] = rows_ref[...]
+    spread_start(0)
     for c in range(2):
         for way in range(2):
             gather_copy(1, way, c).start()
@@ -328,11 +533,43 @@
     dispatch(1)
     for load in loads:
         load.wait()
+    spread_turn(0)
+    blocks = mix_all.shape[0] // BLOCK
 
     @pl.loop(2, half - 1)
     def _(k):
         step(k)
+
+        @pl.when(k == 2)
+        def _():
+            spread_end(0)
+            project()
+            spread_start(1)
+
         experts_on(k - 1)
+
+        @pl.when(k == 3)
+        def _():
+            spread_turn(1)
+
+        @pl.when((k == 3) | (k == 4))
+        def _():
+            scan_blocks((k - 3) * (blocks // 2), (k - 2) * (blocks // 2))
+
+        @pl.when(k == 4)
+        def _():
+            states_out()
+
+        @pl.when(k == 5)
+        def _():
+            scan_open()
+            spread_end(1)
+            shared()
+
+        @pl.when(k == 6)
+        def _():
+            scan_step(0)
+            fold_turn(1)
 
     last = half - 1
     for c in range(2):
@@ -345,11 +582,13 @@
     meta_copy(half, 0).start()
     dispatch(last)
     experts_on(last - 1)
+    scan_step(1)
     for c in range(2):
         gather_copy(half, c, c).wait_recv()
     meta_copy(half, 0).wait_recv()
     dispatch(0)
     experts_on(last)
+    scan_step(2)
     experts_on(0)
 
     def combined(k, span):
@@ -393,6 +632,7 @@
     returned(last)
     for c in range(2):
         pass_on(last, c, lambda way, c: way == c)
+    scan_step(3)
 
     @pl.loop(1, last)
     def _(n):
@@ -401,12 +641,37 @@
         for c in range(2):
             pass_on(k, c, lambda way, c: True)
 
+        @pl.when(n == 1)
+        def _():
+            scan_step(4)
+
+        @pl.when(n == 2)
+        def _():
+            finish_mixer()
+
+        @pl.when(n == 4)
+        def _():
+            fold_turn(0)
+
+    for c in range(2):
+        mixed_ref[:, columns(c)] = fold_end(0, c).astype(jnp.bfloat16)
+        own_sum[:, columns(c)] += fold_end(1, c)
+
     for c in range(2):
         total = own_sum[:, columns(c)]
         for way in range(2):
             sum_copy(1, way, c).wait_recv()
             total = total + sums[way, 0, :, columns(c)].astype(jnp.float32)
-        out_ref[:, columns(c)] = total
+        out_ref[:, columns(c)] = total.astype(jnp.bfloat16)
+
+    spread_sent(1)
+    for which in range(2):
+        fold_sent(which)
+    for part in range(3):
+        mate_copy(part).wait_send()
+    for number in range(len(reaches) + 1):
+        for copy in scan_copies(number):
+            copy.wait_send()
 
     for c in range(2):
         for way in range(2):
@@ -434,26 +699,34 @@
             back_copy(k, i).wait_send()
 
 
-def routed(mesh_sizes, rows, ids, weights, w_gate, w_lift, w_drop):
+def fused(
+    mesh_sizes, mix_normed, rows, ids, weights, shift, decay_cols, bias_cols, head_gain,
+    w_gate, w_lift, w_drop, w_query, w_key, w_value, w_lowrank, w_output,
+    shared_gate, shared_lift, shared_drop,
+):
     nz, nc, nx = mesh_sizes
     half, peers = nz // 2, nc * nx
     tokens, width = rows.shape
     ff = w_gate.shape[-1]
     cap = 2 * tokens * ids.shape[1] // (nz * peers)
     slots = 2 * cap
+    span = nx * tokens
+    keys, values = w_query.shape[1], w_value.shape[1]
+    dv = values * DK // keys
+    scans = len([d for d in (1, 2, 4, 8, 16, 32) if d < nz]) + 1
     meta = jnp.concatenate([ids.T.astype(jnp.float32), weights.T], axis=0)
     vmem, dma = pltpu.VMEM, pltpu.SemaphoreType.DMA
-    bf = jnp.bfloat16
+    bf, f32 = jnp.bfloat16, jnp.float32
     whole = pl.BlockSpec(memory_space=pltpu.VMEM)
     anywhere = pl.BlockSpec(memory_space=pl.ANY)
     return pl.pallas_call(
         functools.partial(moe_kernel, nz, nc, nx),
-        out_shape=jax.ShapeDtypeStruct((tokens, width), jnp.float32),
-        in_specs=[whole, whole, anywhere, anywhere, anywhere],
-        out_specs=whole,
+        out_shape=(jax.ShapeDtypeStruct((tokens, width), bf),) * 2,
+        in_specs=[whole] * 7 + [anywhere] * 11,
+        out_specs=(whole, whole),
         scratch_shapes=[
             vmem((half, 2 * tokens, width), bf),
-            vmem((half, 16, tokens), jnp.float32),
+            vmem((half, 16, tokens), f32),
             vmem((half, peers * slots, 2 * tokens), bf),
             vmem((half, peers * slots, width), bf),
             vmem((half, peers * slots, width), bf),
@@ -464,22 +737,62 @@
             vmem((width, ff), bf),
             vmem((width, ff), bf),
             vmem((ff, width), bf),
+            vmem((width, keys), bf),
+            vmem((width, keys), bf),
+            vmem((width, values), bf),
+            vmem(w_lowrank.shape, bf),
+            vmem((values, width), bf),
+            vmem(shared_gate.shape, bf),
+            vmem(shared_lift.shape, bf),
+            vmem(shared_drop.shape, bf),
             vmem((peers * slots, ff), bf),
-            vmem((tokens, width), jnp.float32),
+            vmem((tokens, width), f32),
+            vmem((span, width), bf),
+            vmem((span, width), bf),
+            vmem((span, width), bf),
+            vmem((2, 2, tokens, width), bf),
+            vmem((2, 2, tokens, width), bf),
+            vmem((span, keys), bf),
+            vmem((span, keys), bf),
+            vmem((span, values), bf),
+            vmem((span, keys), f32),
+            vmem((span, values), f32),
+            vmem((span, keys), bf),
+            vmem((values, keys), f32),
+            vmem((8, keys), f32),
+            vmem((dv, keys), bf),
+            vmem((8, keys), f32),
+            vmem((dv, keys), bf),
+            vmem((8, keys), f32),
+            vmem((dv // 2, keys), f32),
+            vmem((8, keys), f32),
+            vmem((scans + 1, dv // 2, keys), bf),
+            vmem((scans, 8, keys), f32),
+            vmem((scans, dv // 2, keys), bf),
+            vmem((scans, 8, keys), f32),
+            vmem((dv, keys), bf),
             dma((2, half + 1, 2)), dma((2, half + 1, 2)),
             dma((2, half + 1)), dma((2, half + 1)),
             dma((half, peers)), dma((half, peers)),
             dma((half, peers)), dma((half, peers)),
             dma((2, half + 1, 2)), dma((2, half + 1, 2)),
-            dma((3,)),
+            dma((11,)),
+            dma((2, 3, 2, 2)), dma((2, 3, 2, 2)),
+            dma((2, 3, 2, 2)), dma((2, 3, 2, 2)),
+            dma((3,)), dma((3,)),
+            dma((scans, 2)), dma((scans, 2)),
         ],
         compiler_params=pltpu.CompilerParams(
-            collective_id=0, has_side_effects=True, vmem_limit_bytes=58 * 1024 * 1024
+            collective_id=0, has_side_effects=True, vmem_limit_bytes=63 * 1024 * 1024
         ),
         cost_estimate=pl.CostEstimate(
             flops=200_000_000_000, bytes_accessed=16 * 2**20, transcendentals=0
         ),
-    )(rows, meta, w_gate[0], w_lift[0], w_drop[0])
+    )(
+        mix_normed, rows, meta, shift, decay_cols, bias_cols, head_gain,
+        w_gate[0], w_lift[0], w_drop[0], w_query, w_key, w_value, w_lowrank, w_output,
+        shared_gate, shared_lift, shared_drop,
+    )
 
 
 def body(
@@ -508,74 +821,17 @@
     mix_normed = layer_norm(mix_rows, mix_gain)
     local_heads = w_query.shape[1] // DK
     key_cols = local_heads * DK
-    value_cols = w_value.shape[1]
     column = lax.axis_index("tp") * key_cols
     decay_cols = lax.dynamic_slice_in_dim(w_decay, column, key_cols, 1)
     bias_cols = lax.dynamic_slice_in_dim(decay_bias, column, key_cols, 0)
-    shard_rows = lax.all_gather(mix_normed, "tp", axis=0, tiled=True)
-    query_part = jnp.dot(shard_rows, w_query, preferred_element_type=jnp.float32)
-    key_part = jnp.dot(shard_rows, w_key, preferred_element_type=jnp.float32)
-    value_part = jnp.dot(shard_rows, w_value, preferred_element_type=jnp.float32)
-    lowrank = jnp.dot(shard_rows, w_lowrank, preferred_element_type=jnp.float32).astype(
-        jnp.bfloat16
+    expert_normed = layer_norm(expert_rows, ffn_gain)
+    shift = jnp.repeat(jnp.transpose(decay_shift), DK, axis=1)
+    sizes = (lax.axis_size("ep_0"), lax.axis_size("ep_1"), lax.axis_size("tp"))
+    return fused(
+        sizes, mix_normed, expert_normed, route_ids, route_weights, shift, decay_cols,
+        bias_cols[None], head_gain[None], w_gate, w_lift, w_drop, w_query, w_key, w_value,
+        w_lowrank, w_output, shared_gate, shared_lift, shared_drop,
     )
-    logits = jnp.dot(lowrank, decay_cols, preferred_element_type=jnp.float32) + bias_cols
-    projected = jnp.concatenate(
-        [stored(query_part), stored(key_part), stored(value_part), logits], axis=1
-    )
-    span_rows = projected.shape[0]
-    queries = projected[:, :key_cols].reshape(span_rows, local_heads, DK) * DK ** (-0.5)
-    key_rows = projected[:, key_cols : 2 * key_cols].reshape(span_rows, local_heads, DK)
-    value_rows = projected[:, 2 * key_cols : 2 * key_cols + value_cols].reshape(
-        span_rows, local_heads, DV
-    )
-    log_decay = (
-        jax.nn.log_sigmoid(projected[:, 2 * key_cols + value_cols :]).reshape(
-            span_rows, local_heads, DK
-        )
-        / gate_norm
-        + jnp.transpose(decay_shift)[:, :, None]
-    )
-    zero_state = jnp.zeros((local_heads, DK, DV), jnp.float32)
-    inside, final_state, carried_query, decay_total = gla_blocks(
-        queries, key_rows, value_rows, log_decay, zero_state
-    )
-
-    def chain(earlier, later):
-        return (earlier[0] + later[0], jnp.exp(later[0])[:, :, None] * earlier[1] + later[1])
-
-    carried = carried_in(
-        (decay_total, final_state), EP, chain, (jnp.zeros_like(decay_total), zero_state)
-    )
-    entering = carried[1]
-    attended = inside + jnp.einsum("rhd,hdv->rhv", carried_query, entering, precision=highest)
-    inverse = lax.rsqrt(jnp.mean(attended * attended, axis=-1, keepdims=True) + epsilon)
-    head_rows = (
-        (attended * inverse * head_gain).astype(jnp.bfloat16).reshape(span_rows, local_heads * DV)
-    )
-    mixed = lax.psum_scatter(
-        jnp.dot(head_rows, w_output, preferred_element_type=jnp.float32).astype(jnp.bfloat16),
-        "tp",
-        scatter_dimension=0,
-        tiled=True,
-    )
-    expert_normed = layer_norm(expert_rows, ffn_gain)
-    shard_rows = lax.all_gather(expert_normed, "tp", axis=0, tiled=True)
-    hidden = (
-        jax.nn.silu(jnp.dot(shard_rows, shared_gate, preferred_element_type=jnp.float32))
-        * jnp.dot(shard_rows, shared_lift, preferred_element_type=jnp.float32)
-    ).astype(jnp.bfloat16)
-    shared_sum = lax.psum_scatter(
-        jnp.dot(hidden, shared_drop, preferred_element_type=jnp.float32).astype(jnp.bfloat16),
-        "tp",
-        scatter_dimension=0,
-        tiled=True,
-    ).astype(jnp.float32)
-    sizes = (lax.axis_size("ep_0"), lax.axis_size("ep_1"), lax.axis_size("tp"))
-    combined = shared_sum + routed(
-        sizes, expert_normed, route_ids, route_weights, w_gate, w_lift, w_drop
-    )
-    return (mixed, combined.astype(jnp.bfloat16))
 
 
 def solution(mesh):

time: 406 us -> 285 us (0.70)
  waiting for transfers between devices: 78.6 us -> 0 us
  Pallas kernels: 217 us -> 269 us
  blocking collectives: 35.7 us -> 0 us
  matrix products: 23.5 us -> 0 us
  other arithmetic: 26.1 us -> 7.04 us
  between operations: 14.2 us -> 0.76 us
    all_gather x2 -> x0, waiting for transfers between devices: 78.3 us -> none  [the longest x1 46.7 us: body(): shard_rows = lax.all_gather(expert_normed, 'tp', axis=0, tiled=True)]
    pallas_call x1, Pallas kernels: 217 us -> 269 us  [fused(): pl.pallas_call(functools.partial(moe_kernel, nz, nc, nx), out_shape=(jax....]
    all_gather x2 -> x0, blocking collectives: 35.7 us -> none  [gathered_once(): both, at, found = (lax.all_gather(jnp.concatenate(lines), axis), 0, {})]
    dot_general x12 -> x0, matrix products: 23.5 us -> none  [the longest x1 4.86 us: body(): jnp.dot(hidden, shared_drop, preferred_element_type=jnp.float32)]
    add x8 -> x0, other arithmetic: 7.44 us -> none  [advance(): return (jnp.exp(decay_sum)[:, :, None] * state + addition, state)]
    dynamic_update_slice x8 -> x0, other arithmetic: 5.04 us -> none  [gla_blocks(): lax.scan(advance, state_init, (block_total, block_added))]
    unnamed x28 -> x21, local copies, waits for them, and re-layouts: 0.07 us -> 4.81 us
  transfers between devices with their start and end apart: 4 -> 0, of which waited for: 2 -> 0; matrix products, arithmetic and copies ran while one was open for 13% -> 0% of each run, Pallas kernels for 53% -> 0%
where the time goes in v2:
time: 285 us; the launch traced here: 284 us
  Pallas kernels  269 us (94%)
  local copies, waits for them, and re-layouts  7.71 us (3%)
  other arithmetic  7.04 us (2%)
    pallas_call x1, Pallas kernels, fused(): pl.pallas_call(functools.partial(moe_kernel, nz, nc, nx), out_shape=(jax....  269 us

profile of v2, /device:TPU:40, one launch (start us, length us, event | category | flops | bytes accessed | tf_op | source)
XLA Modules:
  0.0 284.2 jit_solution(1619684691234604993)
XLA Ops:
  0.6 0.0 copy-start
  0.6 0.0 copy-start.1
  0.7 0.0 copy-start.2
  0.7 0.0 copy-start.8
  0.7 0.0 copy-start.7
  0.7 0.0 copy-start.6
  0.7 0.0 copy-start.3
  0.7 0.0 copy-start.4
  0.7 0.0 copy-start.5
  0.7 1.5 dynamic-slice_bitcast_fusion.bias_ref
  2.2 1.2 convert_reduce_fusion.1
  3.4 1.3 fusion.7
  4.7 1.2 convert_reduce_fusion
  5.9 1.3 fusion.4
  7.3 0.0 copy-done.7
  7.3 0.0 copy-done.8
  7.3 0.6 pad_maximum_fusion.meta_ref
  7.9 0.0 copy-done
  7.9 0.6 constant_dynamic-slice_fusion.decay_ref
  8.5 0.0 copy-done.6
  8.5 0.8 copy.25.shift_ref
  9.4 0.0 copy-done.3
  9.4 1.0 copy.26.low_hbm
  10.4 0.0 copy-done.1
  10.4 0.0 copy-done.2
  10.4 0.0 copy-done.4
  10.4 0.0 copy-done.5
  10.4 1.4 fusion.6
  11.7 268.7 %shard_map.212 = (bf16[128,2048]{1,0:T(8,128)(2,1)}, bf16[128,2048]{1,0:T(8,128)(2,1)}) custom-call(bf16[128,2048]{1,0:T(8,128)(2,1)} %get-tuple-element.3.mix_ref, bf16[128,2048]{1,0:T(8,128)(2,1)} %get-tuple-element.2.rows_ref, f32[8,128]{1,0:T(8,128)} %pad_maximum_fusion.meta_ref, f32[512,128]{1,0:T(8,128)} %copy.25.shift_ref, ...), custom_call_target="tpu_custom_call" | custom-call | flops 199999995904 | bytes 16777216 | tf_op jit(solution)/shard_map/pallas_call | solution.py:722
  280.4 1.9 copy.29
  282.3 1.9 copy.30
  (6 shorter events, 0.1 us)
Async XLA Ops:
  0.6 7.3 %copy-start = (bf16[32,512]{1,0:T(8,128)(2,1)S(1)}, bf16[32,512]{1,0:T(8,128)(2,1)}, u32[]{:S(2)}) copy-start(bf16[32,512]{1,0:T(8,128)(2,1)} %param.29) | copy-start | bytes 98308
  0.6 9.7 %copy-start.1 = (bf16[128,2048]{1,0:T(8,128)(2,1)S(1)}, bf16[128,2048]{1,0:T(8,128)(2,1)}, u32[]{:S(2)}) copy-start(bf16[128,2048]{1,0:T(8,128)(2,1)} %param.22) | copy-start | bytes 1572868
  0.7 9.7 %copy-start.2 = (bf16[128,2048]{1,0:T(8,128)(2,1)S(1)}, bf16[128,2048]{1,0:T(8,128)(2,1)}, u32[]{:S(2)}) copy-start(bf16[128,2048]{1,0:T(8,128)(2,1)} %param.21) | copy-start | bytes 1572868
  0.7 6.6 %copy-start.8 = (f32[128,4]{0,1:T(4,128)S(1)}, f32[128,4]{0,1:T(4,128)}, u32[]{:S(2)}) copy-start(f32[128,4]{0,1:T(4,128)} %param.35) | copy-start | bytes 6148
  0.7 6.6 %copy-start.7 = (s32[128,4]{0,1:T(4,128)S(1)}, s32[128,4]{0,1:T(4,128)}, u32[]{:S(2)}) copy-start(s32[128,4]{0,1:T(4,128)} %param.34) | copy-start | bytes 6148
  0.7 7.8 %copy-start.6 = (f32[2,512]{1,0:T(2,128)S(1)}, f32[2,512]{1,0:T(2,128)}, u32[]{:S(2)}) copy-start(f32[2,512]{1,0:T(2,128)} %param.31) | copy-start | bytes 12292
  0.7 8.7 %copy-start.3 = (bf16[2048,32]{0,1:T(8,128)(2,1)S(1)}, bf16[2048,32]{0,1:T(8,128)(2,1)}, u32[]{:S(2)}) copy-start(bf16[2048,32]{0,1:T(8,128)(2,1)} %param.28) | copy-start | bytes 393220
  0.7 9.7 %copy-start.4 = (f32[2048]{0:T(1024)S(1)}, f32[2048]{0:T(1024)}, u32[]{:S(2)}) copy-start(f32[2048]{0:T(1024)} %param.24) | copy-start | bytes 24580
  0.7 9.7 %copy-start.5 = (f32[2048]{0:T(1024)S(1)}, f32[2048]{0:T(1024)}, u32[]{:S(2)}) copy-start(f32[2048]{0:T(1024)} %param.23) | copy-start | bytes 24580

commit v3 on v2

--- a/solution.py
+++ b/solution.py
@@ -41,7 +41,8 @@
 
 def moe_kernel(
     nz, nc, nx,
-    mix_ref, rows_ref, meta_ref, shift_ref, decay_ref, bias_ref, gain_ref,
+    mix_ref, rows_ref, mix_gain_ref, ffn_gain_ref, meta_ref, shift_ref, decay_ref, bias_ref,
+    gain_ref,
     gate_hbm, lift_hbm, drop_hbm, query_hbm, key_hbm, value_hbm, low_hbm, mixout_hbm,
     sgate_hbm, slift_hbm, sdrop_hbm,
     mixed_ref, out_ref,
@@ -95,8 +96,19 @@
     ]
     for load in loads:
         load.start()
-    held[0, 0:tokens] = rows_ref[...]
     metas[0, 0:8] = meta_ref[...]
+    own = pl.multiple_of(col * tokens, tokens)
+    rows_at_once = 16
+
+    @pl.loop(0, tokens // rows_at_once)
+    def _(n):
+        start = pl.multiple_of(n * rows_at_once, rows_at_once)
+        span, there = pl.ds(start, rows_at_once), pl.ds(own + start, rows_at_once)
+        mix_all[there] = layer_norm(mix_ref[span], mix_gain_ref[...])
+        normed = layer_norm(rows_ref[span], ffn_gain_ref[...])
+        held[0, span] = normed
+        exp_all[there] = normed
+
     pl.semaphore_wait(barrier, peers - 1 + len(near))
 
     def place(k, way):
@@ -109,7 +121,7 @@
 
     def gather_copy(k, way, c):
         if isinstance(k, int) and k == 1:
-            source = rows_ref.at[:, columns(c)]
+            source = held.at[0, slice(0, tokens), columns(c)]
         else:
             at, span = place(k - 1, way)
             source = held.at[at, span, columns(c)]
@@ -230,9 +242,11 @@
                 hidden[...], drop_ref[:, span], preferred_element_type=jnp.float32
             ).astype(jnp.bfloat16)
 
+        back[k, block(me)] = results[k, block(me)]
+
+    def back_start(k):
         for i in range(1, peers):
             back_copy(k, i).start()
-        back[k, block(me)] = results[k, block(me)]
 
     side_cols = (lax.rem(col + 1, nx), lax.rem(col + nx - 1, nx))
     turn = nx // 2
@@ -244,11 +258,10 @@
         return pl.ds(pl.multiple_of(number * tokens, tokens), tokens)
 
     def spread_copy(which, k, way, c, landed=False):
-        source, full = (mix_ref, mix_all) if which == 0 else (rows_ref, exp_all)
+        full = mix_all if which == 0 else exp_all
         at = row_block(off(k if landed else k - 1, 1 - way))
         return pltpu.make_async_remote_copy(
-            source.at[:, columns(c)] if k == 1 else full.at[at, columns(c)],
-            full.at[at, columns(c)],
+            full.at[at, columns(c)], full.at[at, columns(c)],
             xg_send.at[which, k, way, c], xg_recv.at[which, k, way, c],
             device_id={"tp": side_cols[way]}, device_id_type=MESH,
         )
@@ -319,6 +332,8 @@
     dv = values // (keys // DK)
     lane_head = lax.broadcasted_iota(jnp.int32, (1, keys), 1) // DK
     head_masks = [jnp.where(lane_head == h, 1.0, 0.0) for h in range(2)]
+
+    lanes = pl.ds(pl.multiple_of(col * keys, keys), keys)
 
     def project():
         @pl.loop(0, mix_all.shape[0] // (2 * tokens))
@@ -332,10 +347,16 @@
             k_rows[span] = key.astype(jnp.bfloat16)
             value = jnp.dot(rows, value_ref[...], preferred_element_type=f32)
             v_rows[span] = value.astype(jnp.bfloat16)
-            low = jnp.dot(rows, low_ref[...], preferred_element_type=f32).astype(jnp.bfloat16)
-            logit = jnp.dot(low, decay_ref[...], preferred_element_type=f32) + bias_ref[...]
+            low = lax.dot_general(
+                rows, low_ref[...], (((1,), (1,)), ((), ())), preferred_element_type=f32
+            ).astype(jnp.bfloat16)
+            logit = jnp.dot(low, decay_ref[:, lanes], preferred_element_type=f32) + bias_ref[:, lanes]
             soft = jnp.minimum(logit, 0.0) - jnp.log1p(jnp.exp(-jnp.abs(logit)))
-            decays[span] = soft * (1.0 / gate_norm) + shift_ref[span]
+            moved = lax.dot_general(
+                shift_ref[:, span], jnp.concatenate(head_masks, axis=0), (((0,), (0,)), ((), ())),
+                precision=highest, preferred_element_type=f32,
+            )
+            decays[span] = soft * (1.0 / gate_norm) + moved
 
         state[...] = jnp.zeros_like(state)
         before[...] = jnp.zeros_like(before)
@@ -502,10 +523,6 @@
                 unit, sdrop_ref[...], preferred_element_type=jnp.float32
             ).astype(jnp.bfloat16)
 
-        fold_start(1)
-
-    mix_all[row_block(col)] = mix_ref[...]
-    exp_all[row_block(col)] = rows_ref[...]
     spread_start(0)
     for c in range(2):
         for way in range(2):
@@ -513,32 +530,31 @@
     for way in range(2):
         meta_copy(1, way).start()
 
-    def step(k):
-        for c in range(2):
-            for way in range(2):
-                gather_copy(k, way, c).wait_recv()
+    def pass_rows(k, c):
+        for way in range(2):
+            gather_copy(k, way, c).wait_recv()
+            if not (isinstance(k, int) and k == half - 1) or way == c:
                 gather_copy(k + 1, way, c).start()
+
+    def pass_meta(k):
         for way in range(2):
             meta_copy(k, way).wait_recv()
-            meta_copy(k + 1, way).start()
-        dispatch(k)
-
+            if not (isinstance(k, int) and k == half - 1) or way == 0:
+                meta_copy(k + 1, way).start()
+
+    last = half - 1
+    blocks = mix_all.shape[0] // BLOCK
     for c in range(2):
-        for way in range(2):
-            gather_copy(1, way, c).wait_recv()
-            gather_copy(2, way, c).start()
-    for way in range(2):
-        meta_copy(1, way).wait_recv()
-        meta_copy(2, way).start()
+        pass_rows(1, c)
+    pass_meta(1)
     dispatch(1)
     for load in loads:
         load.wait()
     spread_turn(0)
-    blocks = mix_all.shape[0] // BLOCK
-
-    @pl.loop(2, half - 1)
+
+    @pl.loop(2, last)
     def _(k):
-        step(k)
+        pass_rows(k, 0)
 
         @pl.when(k == 2)
         def _():
@@ -546,12 +562,6 @@
             project()
             spread_start(1)
 
-        experts_on(k - 1)
-
-        @pl.when(k == 3)
-        def _():
-            spread_turn(1)
-
         @pl.when((k == 3) | (k == 4))
         def _():
             scan_blocks((k - 3) * (blocks // 2), (k - 2) * (blocks // 2))
@@ -569,27 +579,32 @@
         @pl.when(k == 6)
         def _():
             scan_step(0)
-            fold_turn(1)
-
-    last = half - 1
-    for c in range(2):
-        for way in range(2):
-            gather_copy(last, way, c).wait_recv()
-            if way == c:
-                gather_copy(half, way, c).start()
-    for way in range(2):
-        meta_copy(last, way).wait_recv()
-    meta_copy(half, 0).start()
+
+        pass_rows(k, 1)
+        pass_meta(k)
+        dispatch(k)
+        experts_on(k - 1)
+
+        @pl.when(k == 3)
+        def _():
+            spread_turn(1)
+
+    pass_rows(last, 0)
+    scan_step(1)
+    pass_rows(last, 1)
+    pass_meta(last)
     dispatch(last)
     experts_on(last - 1)
-    scan_step(1)
     for c in range(2):
         gather_copy(half, c, c).wait_recv()
     meta_copy(half, 0).wait_recv()
     dispatch(0)
     experts_on(last)
+    back_start(last)
     scan_step(2)
     experts_on(0)
+    back_start(0)
+    back_start(last - 1)
 
     def combined(k, span):
         return lax.dot_general(
@@ -632,7 +647,9 @@
     returned(last)
     for c in range(2):
         pass_on(last, c, lambda way, c: way == c)
+    back_start(last - 2)
     scan_step(3)
+    fold_start(1)
 
     @pl.loop(1, last)
     def _(n):
@@ -641,12 +658,17 @@
         for c in range(2):
             pass_on(k, c, lambda way, c: True)
 
+        @pl.when(k >= 3)
+        def _():
+            back_start(k - 2)
+
         @pl.when(n == 1)
         def _():
             scan_step(4)
 
         @pl.when(n == 2)
         def _():
+            fold_turn(1)
             finish_mixer()
 
         @pl.when(n == 4)
@@ -700,7 +722,8 @@
 
 
 def fused(
-    mesh_sizes, mix_normed, rows, ids, weights, shift, decay_cols, bias_cols, head_gain,
+    mesh_sizes, mix_rows, rows, mix_gain, ffn_gain, ids, weights, shift, w_decay, decay_bias,
+    head_gain,
     w_gate, w_lift, w_drop, w_query, w_key, w_value, w_lowrank, w_output,
     shared_gate, shared_lift, shared_drop,
 ):
@@ -722,7 +745,7 @@
     return pl.pallas_call(
         functools.partial(moe_kernel, nz, nc, nx),
         out_shape=(jax.ShapeDtypeStruct((tokens, width), bf),) * 2,
-        in_specs=[whole] * 7 + [anywhere] * 11,
+        in_specs=[whole] * 9 + [anywhere] * 11,
         out_specs=(whole, whole),
         scratch_shapes=[
             vmem((half, 2 * tokens, width), bf),
@@ -789,7 +812,7 @@
             flops=200_000_000_000, bytes_accessed=16 * 2**20, transcendentals=0
         ),
     )(
-        mix_normed, rows, meta, shift, decay_cols, bias_cols, head_gain,
+        mix_rows, rows, mix_gain, ffn_gain, meta, shift, w_decay, decay_bias, head_gain,
         w_gate[0], w_lift[0], w_drop[0], w_query, w_key, w_value, w_lowrank, w_output,
         shared_gate, shared_lift, shared_drop,
     )
@@ -818,19 +841,12 @@
     shared_lift,
     shared_drop,
 ):
-    mix_normed = layer_norm(mix_rows, mix_gain)
-    local_heads = w_query.shape[1] // DK
-    key_cols = local_heads * DK
-    column = lax.axis_index("tp") * key_cols
-    decay_cols = lax.dynamic_slice_in_dim(w_decay, column, key_cols, 1)
-    bias_cols = lax.dynamic_slice_in_dim(decay_bias, column, key_cols, 0)
-    expert_normed = layer_norm(expert_rows, ffn_gain)
-    shift = jnp.repeat(jnp.transpose(decay_shift), DK, axis=1)
     sizes = (lax.axis_size("ep_0"), lax.axis_size("ep_1"), lax.axis_size("tp"))
     return fused(
-        sizes, mix_normed, expert_normed, route_ids, route_weights, shift, decay_cols,
-        bias_cols[None], head_gain[None], w_gate, w_lift, w_drop, w_query, w_key, w_value,
-        w_lowrank, w_output, shared_gate, shared_lift, shared_drop,
+        sizes, mix_rows, expert_rows, mix_gain[None], ffn_gain[None], route_ids, route_weights,
+        decay_shift, w_decay, decay_bias[None], head_gain[None], w_gate, w_lift, w_drop,
+        w_query, w_key, w_value, jnp.transpose(w_lowrank), w_output,
+        shared_gate, shared_lift, shared_drop,
     )
 
 

time: 285 us -> 249 us (0.87)
  Pallas kernels: 269 us -> 242 us
  other arithmetic: 7.04 us -> 1.96 us
  local copies, waits for them, and re-layouts: 7.71 us -> 3.76 us
    pallas_call x1, Pallas kernels: 269 us -> 242 us  [fused(): pl.pallas_call(functools.partial(moe_kernel, nz, nc, nx), out_shape=(jax....]
    reduce_sum x4 -> x0, other arithmetic: 5.05 us -> none  [the longest x2 2.66 us: layer_norm(): jnp.mean(center * center, axis=-1, keepdims=True) + epsilon]
where the time goes in v3:
time: 249 us; the launch traced here: 248 us
  Pallas kernels  242 us (97%)
  local copies, waits for them, and re-layouts  3.76 us (2%)
    pallas_call x1, Pallas kernels, fused(): pl.pallas_call(functools.partial(moe_kernel, nz, nc, nx), out_shape=(jax....  242 us

profile of v3, /device:TPU:40, one launch (start us, length us, event | category | flops | bytes accessed | tf_op | source)
XLA Modules:
  0.0 248.4 jit_solution(2021125642443977376)
XLA Ops:
  0.6 0.7 convert_bitcast_fusion
  1.3 1.3 pad_maximum_fusion.meta_ref
  2.6 242.1 %shard_map.212 = (bf16[128,2048]{1,0:T(8,128)(2,1)}, bf16[128,2048]{1,0:T(8,128)(2,1)}) custom-call(bf16[128,2048]{1,0:T(8,128)(2,1)} %mix_ref.1, bf16[128,2048]{1,0:T(8,128)(2,1)} %rows_ref.1, f32[1,2048]{1,0:T(1,128)} %bitcast.16, f32[1,2048]{1,0:T(1,128)} %bitcast.17, f32[8,128]{1,0:T(8,128)} %pad_maximum_fusion.meta_ref, f32[2,512]{1,0:T(2,128)} %shift_ref.1, ...), custom_call_target="tpu_custom_call" | custom-call | flops 199999995904 | bytes 16777216 | tf_op jit(solution)/shard_map/pallas_call | solution.py:745
  244.7 1.9 copy.25
  246.5 1.9 copy.26
